TPU v7x, 32 devices: a whole 2x2x4 slice. The times are simulated.
32 devices in a mesh: sp: 8 (over z, x), tp: 4 (over y, core).
Axes of the slice: x: 2, y: 2, z: 4, core: 2. Of those that a mesh axis runs over, the one named last changes fastest.
Arguments:
- cotangent: bfloat16 [1024, 2048], P('sp'), may hold values from -6 to 6
- stream: bfloat16 [1024, 2048], P('sp'), may hold values from -6 to 6
- routes: int32 [1024, 2], P('sp'), may hold values from 0 to 3, all different within a row; in each aligned block of 128 rows (0 to 127, 128 to 255, ...) at most 96 rows name the same one
- route_weights: float32 [1024, 2], P('sp'), may hold values from 0.25 to 1
- gate_weight: bfloat16 [8, 2048, 2048], P('sp', None, 'tp'), may hold values from -0.125 to 0.125
- up_weight: bfloat16 [8, 2048, 2048], P('sp', None, 'tp'), may hold values from -0.125 to 0.125
- down_weight: bfloat16 [8, 2048, 2048], P('sp', 'tp'), may hold values from -0.09375 to 0.09375
- outer_gate: bfloat16 [1024, 1024], P('sp', 'tp'), may hold values from -6 to 6
- inner_gate: bfloat16 [1024, 1024], P('sp', 'tp'), may hold values from -6 to 6
- conv_input: bfloat16 [1024, 1024], P('sp', 'tp'), may hold values from -6 to 6
- conv_taps: bfloat16 [3, 1024], P(None, 'tp'), may hold values from -1 to 1
- out_weight: bfloat16 [2048, 1024], P(None, 'tp'), may hold values from -0.1875 to 0.1875
Outputs:
- gate_grad: bfloat16 [8, 2048, 2048], P('sp', None, 'tp')
- up_grad: bfloat16 [8, 2048, 2048], P('sp', None, 'tp')
- down_grad: bfloat16 [8, 2048, 2048], P('sp', 'tp')
- out_grad: float32 [2048, 1024], P('sp', 'tp')
- outer_grad: bfloat16 [1024, 1024], P('sp', 'tp')
- inner_grad: bfloat16 [1024, 1024], P('sp', 'tp')
- input_grad: bfloat16 [1024, 1024], P('sp', 'tp')
Inputs may be any that keep to these rules, and one draw needn't show every extreme that they name: `routes`: each token names two different experts. Among the 128 tokens of one index of sp no expert is named by more than 96 tokens, a bound that some block of them reaches in every draw.
All inputs are finite; a program needn't handle non-finite values.
Results may differ from a plain program's by a relative error of at most 0.02.
Values may be sent and summed in bfloat16 or wider, within the bound.
A program may use at most 64 MiB of HBM per device.

v0:
```python
import jax
import jax.numpy as jnp
from jax import lax
from jax.sharding import PartitionSpec as P


def from_behind(block, axis, distance):
    devices = range(lax.axis_size(axis))
    route = [(i - distance, i) for i in devices if i - distance in devices]
    return lax.ppermute(block, axis, route)


def per_device(
    cotangent,
    stream,
    routes,
    route_weights,
    gate_weight,
    up_weight,
    down_weight,
    outer_gate,
    inner_gate,
    conv_input,
    conv_taps,
    out_weight,
):
    groups = lax.axis_size("sp")
    tp_count = lax.axis_size("tp")
    experts = groups // 2
    tok_rows = stream.shape[0]
    model_width = stream.shape[1]
    capacity = 3 * tok_rows // experts
    slot_total = experts * capacity
    contract_first = (((0,), (0,)), ((), ()))
    contract_last = (((1,), (1,)), ((), ()))
    flat_routes = routes.reshape(-1)
    choose = (flat_routes[:, None] == jnp.arange(experts, dtype=jnp.int32)[None, :]).astype(
        jnp.int32
    )
    before = jnp.cumsum(choose, axis=0) - choose
    slot_place = flat_routes * capacity + jnp.sum(before * choose, axis=1)
    slot_table = (jnp.arange(slot_total, dtype=jnp.int32)[:, None] == slot_place[None, :]).astype(
        jnp.float32
    )
    select = jnp.sum(slot_table.reshape(slot_total, tok_rows, 2), axis=2).astype(jnp.bfloat16)
    slot_weight = jnp.sum(slot_table * route_weights.reshape(-1)[None, :], axis=1)
    block_width = model_width // tp_count
    offset = lax.axis_index("tp") * block_width
    rows_part = lax.dynamic_slice_in_dim(stream, offset, block_width, 1)
    cot_part = lax.dynamic_slice_in_dim(cotangent, offset, block_width, 1)
    sent_rows = jnp.dot(select, rows_part, preferred_element_type=jnp.float32).astype(jnp.bfloat16)
    sent_cot = (
        jnp.dot(select, cot_part, preferred_element_type=jnp.float32) * slot_weight[:, None]
    ).astype(jnp.bfloat16)
    sent_rows = jnp.repeat(sent_rows.reshape(experts, capacity, -1), 2, axis=0)
    sent_cot = jnp.repeat(sent_cot.reshape(experts, capacity, -1), 2, axis=0)
    recv_rows, recv_cot = (
        lax.all_to_all(sent_rows, "sp", split_axis=0, concat_axis=0, tiled=True),
        lax.all_to_all(sent_cot, "sp", split_axis=0, concat_axis=0, tiled=True),
    )
    recv_rows, recv_cot = (
        lax.all_gather(recv_rows, "tp", axis=2, tiled=True),
        lax.all_gather(recv_cot, "tp", axis=2, tiled=True),
    )
    slots = groups * capacity
    routed_rows = recv_rows.reshape(slots, model_width)
    routed_cot = recv_cot.reshape(slots, model_width)
    gate_local = gate_weight[0]
    up_local = up_weight[0]
    down_local = down_weight[0]
    gate_pre = jnp.dot(routed_rows, gate_local, preferred_element_type=jnp.float32)
    up_pre = jnp.dot(routed_rows, up_local, preferred_element_type=jnp.float32)
    hidden_grad = lax.dot_general(
        routed_cot, down_local, contract_last, preferred_element_type=jnp.float32
    )
    sigma = jax.nn.sigmoid(gate_pre)
    silu_gate = gate_pre * sigma
    hidden = (silu_gate * up_pre).astype(jnp.bfloat16)
    up_delta = (hidden_grad * silu_gate).astype(jnp.bfloat16)
    gate_delta = (hidden_grad * up_pre * sigma * (1.0 + gate_pre * (1.0 - sigma))).astype(
        jnp.bfloat16
    )
    gate_grad = lax.dot_general(
        routed_rows, gate_delta, contract_first, preferred_element_type=jnp.float32
    ).astype(jnp.bfloat16)[None]
    up_grad = lax.dot_general(
        routed_rows, up_delta, contract_first, preferred_element_type=jnp.float32
    ).astype(jnp.bfloat16)[None]
    down_grad = lax.dot_general(
        hidden, routed_cot, contract_first, preferred_element_type=jnp.float32
    ).astype(jnp.bfloat16)[None]
    row_partial = lax.dot_general(
        gate_delta, gate_local, contract_last, preferred_element_type=jnp.float32
    )
    row_partial = row_partial + lax.dot_general(
        up_delta, up_local, contract_last, preferred_element_type=jnp.float32
    )
    half_sums = lax.psum_scatter(
        row_partial.astype(jnp.bfloat16), "tp", scatter_dimension=1, tiled=True
    ).astype(jnp.float32)
    block_width = half_sums.shape[1]
    half_grad = half_sums.reshape(groups, capacity, block_width).astype(jnp.bfloat16)
    returned = lax.all_to_all(half_grad, "sp", split_axis=0, concat_axis=0, tiled=True)
    returned = returned.reshape(experts, 2, capacity, block_width)
    select_three = select.reshape(experts, capacity, tok_rows)
    moe_part = jnp.einsum(
        "ecr,emcd->rd", select_three, returned, preferred_element_type=jnp.float32
    ).astype(jnp.bfloat16)
    moe_grad = lax.all_gather(moe_part, "tp", axis=1, tiled=True)
    stream_grad = (cotangent.astype(jnp.float32) + moe_grad.astype(jnp.float32)).astype(
        jnp.bfloat16
    )
    taps = conv_taps.astype(jnp.float32)
    outer_f = outer_gate.astype(jnp.float32)
    inner_f = inner_gate.astype(jnp.float32)
    input_f = conv_input.astype(jnp.float32)
    mixed = inner_f * input_f
    earlier = from_behind(mixed[-2:], "sp", 1)
    padded = jnp.concatenate([earlier, mixed], axis=0)
    conv_sum = taps[0] * padded[:-2] + taps[1] * padded[1:-1] + taps[2] * padded[2:]
    conv_out = (outer_f * conv_sum).astype(jnp.bfloat16)
    out_grad = lax.psum_scatter(
        lax.dot_general(
            stream_grad, conv_out, contract_first, preferred_element_type=jnp.float32
        ).astype(jnp.bfloat16),
        "sp",
        scatter_dimension=0,
        tiled=True,
    ).astype(jnp.float32)
    conv_grad = jnp.dot(stream_grad, out_weight, preferred_element_type=jnp.float32)
    outer_grad = (conv_grad * conv_sum).astype(jnp.bfloat16)
    scaled = conv_grad * outer_f
    later = from_behind(scaled[:2], "sp", -1)
    extended = jnp.concatenate([scaled, later], axis=0)
    mixed_grad = taps[2] * extended[:-2] + taps[1] * extended[1:-1] + taps[0] * extended[2:]
    inner_grad = (mixed_grad * input_f).astype(jnp.bfloat16)
    input_grad = (mixed_grad * inner_f).astype(jnp.bfloat16)
    return (gate_grad, up_grad, down_grad, out_grad, outer_grad, inner_grad, input_grad)


def solution(mesh):
    placed = (
        P("sp", None),
        P("sp", None),
        P("sp", None),
        P("sp", None),
        P("sp", None, "tp"),
        P("sp", None, "tp"),
        P("sp", "tp", None),
        P("sp", "tp"),
        P("sp", "tp"),
        P("sp", "tp"),
        P(None, "tp"),
        P(None, "tp"),
    )
    return jax.shard_map(
        per_device,
        mesh=mesh,
        in_specs=placed,
        out_specs=(
            P("sp", None, "tp"),
            P("sp", None, "tp"),
            P("sp", "tp", None),
            P("sp", "tp"),
            P("sp", "tp"),
            P("sp", "tp"),
            P("sp", "tp"),
        ),
        check_vma=False,
    )
```

profile of v0, /device:TPU:0, one launch (start us, length us, event | category | flops | bytes accessed | tf_op | source)
XLA Modules:
  0.0 253.2 jit_solution(881290032400397519)
XLA Ops:
  7.2 0.9 copy.37
  8.2 0.1 eq.50
  8.3 0.1 eq.46
  8.5 1.2 reduce-window.6
  9.7 0.1 slice.47
  9.8 0.1 copy.39
  9.9 0.1 copy.40
  10.0 0.1 add_bitcast_fusion
  10.1 0.1 reduce_sum.39
  10.2 0.1 copy.41
  10.3 0.7 multiply_add_fusion.1
  11.0 0.1 convert_reduce_fusion.1
  11.1 1.2 convolution_convert_fusion.4
  12.3 0.1 broadcast_in_dim.19
  12.4 27.3 %all_to_all.15 = bf16[8,96,512]{2,1,0:T(8,128)(2,1)} all-to-all(bf16[8,96,512]{2,1,0:T(8,128)(2,1)S(1)} %bitcast.73), channel_id=1, replica_groups=mesh['sp'=8,'tp'=4] {'sp'}, dimensions={0} | all-to-all | bytes 1572864 | tf_op jit(solution)/shard_map/all_to_all | solution.py:58
  39.8 0.1 copy.42
  39.9 0.1 mul.132
  40.1 0.1 select_reduce_fusion
  40.2 0.3 fusion.13
  40.5 0.1 broadcast_in_dim.20
  40.6 23.3 %all_to_all.16 = bf16[8,96,512]{2,1,0:T(8,128)(2,1)} all-to-all(bf16[8,96,512]{2,1,0:T(8,128)(2,1)S(1)} %bitcast.74), channel_id=1, replica_groups=mesh['sp'=8,'tp'=4] {'sp'}, dimensions={0} | all-to-all | bytes 1572864 | tf_op jit(solution)/shard_map/all_to_all | solution.py:59
  63.9 3.5 %all-gather.3.cloned.1.call-done = bf16[8,96,2048]{2,1,0:T(8,128)(2,1)} async-done(((bf16[8,96,512]{2,1,0:T(8,128)(2,1)}), bf16[8,96,2048]{2,1,0:T(8,128)(2,1)}) %all-gather.3.cloned.1.call-update) | async-done | bytes 3145744 | tf_op jit(solution)/shard_map/all_gather | solution.py:62
  67.4 5.0 %fusion.5 = f32[768,512]{1,0:T(8,128)} fusion(bf16[768,2048]{1,0:T(8,128)(2,1)} %bitcast.86, bf16[1,2048,512]{2,1,0:T(8,128)(2,1)S(1)} %copy-done), kind=kOutput, calls=%fused_computation.10 | convolution fusion | flops 1610612736 | bytes 6815744 | tf_op jit(solution)/shard_map/dot_general | solution.py:71
  72.4 2.9 %fusion.8 = f32[768,512]{1,0:T(8,128)} fusion(bf16[768,2048]{1,0:T(8,128)(2,1)S(1)} %bitcast.88, bf16[1,2048,512]{2,1,0:T(8,128)(2,1)S(1)} %copy-done.2), kind=kOutput, calls=%fused_computation.13 | convolution fusion | flops 1610612736 | bytes 6815744 | tf_op jit(solution)/shard_map/dot_general | solution.py:72
  75.3 22.2 %all-gather.5.cloned.1.call-done = bf16[8,96,2048]{2,1,0:T(8,128)(2,1)} async-done(((bf16[8,96,512]{2,1,0:T(8,128)(2,1)}), bf16[8,96,2048]{2,1,0:T(8,128)(2,1)}) %all-gather.5.cloned.1.call-update) | async-done | bytes 3145744 | tf_op jit(solution)/shard_map/all_gather | solution.py:63
  97.5 5.7 %multiply_convert_fusion.1 = (bf16[768,512]{1,0:T(8,128)(2,1)S(1)}, bf16[768,512]{1,0:T(8,128)(2,1)S(1)}) fusion(f32[768,512]{1,0:T(8,128)} %fusion.5, f32[768,512]{1,0:T(8,128)} %fusion.8, bf16[768,2048]{1,0:T(8,128)(2,1)} %bitcast.90, bf16[1,512,2048]{2,1,0:T(8,128)(2,1)} %param.18), kind=kOutput, calls=%fused_computation.19 | convolution fusion | flops 1615724544 | bytes 9961472 | tf_op jit(solution)/shard_map/dot_general | solution.py:73
  103.3 1.8 fusion.3
  105.1 0.3 copy-done.3
  105.4 3.5 %add_convert_fusion = bf16[768,2048]{1,0:T(8,128)(2,1)} fusion(f32[768,2048]{1,0:T(8,128)S(1)} %fusion.3, bf16[768,512]{1,0:T(8,128)(2,1)S(1)} %get-tuple-element.11, bf16[1,2048,512]{2,1,0:T(8,128)(2,1)S(1)} %copy-done.3), kind=kOutput, calls=%fused_computation | convolution fusion | flops 1613758464 | bytes 12320768 | tf_op jit(solution)/shard_map/dot_general | solution.py:95
  109.0 37.9 %reduce-scatter.3.cloned.1.call-done = bf16[768,512]{1,0:T(8,128)(2,1)} async-done(((bf16[768,2048]{1,0:T(8,128)(2,1)}), bf16[768,512]{1,0:T(8,128)(2,1)}) %reduce-scatter.3.cloned.1.call-update) | async-done | bytes 786448 | tf_op jit(solution)/shard_map/reduce_scatter | solution.py:98
  146.8 5.5 %all-to-all-start.2 = ((bf16[8,96,512]{2,1,0:T(8,128)(2,1)}), bf16[8,96,512]{2,1,0:T(8,128)(2,1)S(1)}, u32[]{:S(2)}, u32[]{:S(2)}) async-start(bf16[8,96,512]{2,1,0:T(8,128)(2,1)} %bitcast.78), calls=%async_computation.3 | async-start | bytes 1572864 | tf_op jit(solution)/shard_map/all_to_all | solution.py:103
  152.4 0.9 convert_multiply_fusion.1
  153.3 3.9 %collective-permute-start = (f32[2,256]{1,0:T(2,128)S(1)}, f32[2,256]{1,0:T(2,128)S(1)}, u32[]{:S(2)}, u32[]{:S(2)}) collective-permute-start(f32[2,256]{1,0:T(2,128)S(1)} %slice.49), channel_id=1, source_target_pairs={{0,4},{4,8},{8,12},{12,16},{16,20},{20,24},{24,28},{1,5},{5,9},{9,... | collective-permute-start | bytes 6152 | tf_op jit(solution)/shard_map/ppermute | solution.py:10
  157.2 15.2 %all-to-all-done.2 = bf16[8,96,512]{2,1,0:T(8,128)(2,1)S(1)} async-done(((bf16[8,96,512]{2,1,0:T(8,128)(2,1)}), bf16[8,96,512]{2,1,0:T(8,128)(2,1)S(1)}, u32[]{:S(2)}, u32[]{:S(2)}) %all-to-all-start.2) | async-done | bytes 786464 | tf_op jit(solution)/shard_map/all_to_all | solution.py:103
  172.4 0.1 convert_reduce_fusion
  172.6 0.2 fusion.14
  172.8 6.7 %all_gather.11 = bf16[128,2048]{1,0:T(8,128)(2,1)S(1)} all-gather(bf16[128,512]{1,0:T(8,128)(2,1)S(1)} %fusion.14), channel_id=1, replica_groups=mesh['sp'=8,'tp'=4] {'tp'}, dimensions={1}, use_global_device_ids=true | all-gather | bytes 655360 | tf_op jit(solution)/shard_map/all_gather | solution.py:109
  179.5 1.0 multiply_convert_fusion.4
  180.5 1.5 convolution_convert_fusion.3
  182.1 5.2 %fusion = bf16[1,2048,512]{2,1,0:T(8,128)(2,1)} fusion(bf16[768,2048]{1,0:T(8,128)(2,1)} %bitcast.87, bf16[768,512]{1,0:T(8,128)(2,1)S(1)} %copy-done.8), kind=kOutput, calls=%fused_computation.4 | convolution fusion | flops 1611661312 | bytes 6029312 | tf_op jit(solution)/shard_map/dot_general | solution.py:83
  187.3 3.3 %fusion.2 = bf16[1,512,2048]{2,1,0:T(8,128)(2,1)} fusion(bf16[768,2048]{1,0:T(8,128)(2,1)S(1)} %bitcast.91, f32[768,512]{1,0:T(8,128)S(1)} %copy-done.21, f32[768,512]{1,0:T(8,128)S(1)} %copy-done.20), kind=kOutput, calls=%fused_computation.6 | convolution fusion | flops 1614020608 | bytes 8388608 | tf_op jit(solution)/shard_map/dot_general | solution.py:89
  190.6 1.4 collective-permute-start.1
  192.1 3.2 %fusion.1 = bf16[1,2048,512]{2,1,0:T(8,128)(2,1)} fusion(bf16[768,2048]{1,0:T(8,128)(2,1)S(1)} %bitcast.89, bf16[768,512]{1,0:T(8,128)(2,1)S(1)} %copy-done.6), kind=kOutput, calls=%fused_computation.5 | convolution fusion | flops 1611661312 | bytes 6029312 | tf_op jit(solution)/shard_map/dot_general | solution.py:86
  195.3 1.0 collective-permute-done.1
  196.2 0.7 fusion.26
  196.9 0.6 fusion.27
  197.6 47.4 %reduce-scatter.5.cloned.1.call-done = bf16[256,256]{1,0:T(8,128)(2,1)} async-done(((bf16[2048,256]{1,0:T(8,128)(2,1)}), bf16[256,256]{1,0:T(8,128)(2,1)}) %reduce-scatter.5.cloned.1.call-update) | async-done | bytes 131088 | tf_op jit(solution)/shard_map/reduce_scatter | solution.py:122
  245.0 1.6 convert_element_type.125
  (60 shorter events, 0.4 us)
Async XLA Ops:
  7.2 60.3 %copy-start = (bf16[1,2048,512]{2,1,0:T(8,128)(2,1)S(1)}, bf16[1,2048,512]{2,1,0:T(8,128)(2,1)}, u32[]{:S(2)}) copy-start(bf16[1,2048,512]{2,1,0:T(8,128)(2,1)} %param.16) | copy-start | bytes 6291460
  7.2 60.3 %all-gather.3.cloned.1.call-start = ((), (), s32[]{:S(2)}) async-start(), calls=%async_computation.5 | async-start | bytes 3932160 | tf_op jit(solution)/shard_map/all_gather | solution.py:62
  11.1 28.7 %copy-start.16 = (f32[128,2]{0,1:T(2,128)S(1)}, f32[128,2]{0,1:T(2,128)}, u32[]{:S(2)}) copy-start(f32[128,2]{0,1:T(2,128)} %param.15) | copy-start | bytes 3076
  11.1 29.1 %copy-start.1 = (bf16[128,2048]{1,0:T(8,128)(2,1)S(1)}, bf16[128,2048]{1,0:T(8,128)(2,1)}, u32[]{:S(2)}) copy-start(bf16[128,2048]{1,0:T(8,128)(2,1)} %param.12) | copy-start | bytes 1572868
  39.7 57.8 %all-gather.5.cloned.1.call-start = ((), (), s32[]{:S(2)}) async-start(), calls=%async_computation.6 | async-start | bytes 3932160 | tf_op jit(solution)/shard_map/all_gather | solution.py:63
  63.9 83.0 %reduce-scatter.3.cloned.1.call-start = ((), (), s32[]{:S(2)}) async-start(), calls=%async_computation.7 | async-start | bytes 3932160 | tf_op jit(solution)/shard_map/reduce_scatter | solution.py:98
  67.4 5.0 %copy-start.2 = (bf16[1,2048,512]{2,1,0:T(8,128)(2,1)S(1)}, bf16[1,2048,512]{2,1,0:T(8,128)(2,1)}, u32[]{:S(2)}) copy-start(bf16[1,2048,512]{2,1,0:T(8,128)(2,1)} %param.17) | copy-start | bytes 6291460
  67.4 5.0 %copy-start.17 = (bf16[8,96,2048]{2,1,0:T(8,128)(2,1)S(1)}, bf16[8,96,2048]{2,1,0:T(8,128)(2,1)}, u32[]{:S(2)}) copy-start(bf16[8,96,2048]{2,1,0:T(8,128)(2,1)} %all-gather.3.cloned.1.call-done) | copy-start | bytes 9437188
  103.2 1.9 copy-start.7
  103.2 1.9 copy-start.5
  103.3 2.2 copy-start.3
  108.9 48.3 %copy-start.15 = (bf16[3,256]{1,0:T(4,128)(2,1)S(1)}, bf16[3,256]{1,0:T(4,128)(2,1)}, u32[]{:S(2)}) copy-start(bf16[3,256]{1,0:T(4,128)(2,1)} %param.22) | copy-start | bytes 4612
  146.8 25.6 %all-to-all-start.2 = ((bf16[8,96,512]{2,1,0:T(8,128)(2,1)}), bf16[8,96,512]{2,1,0:T(8,128)(2,1)S(1)}, u32[]{:S(2)}, u32[]{:S(2)}) async-start(bf16[8,96,512]{2,1,0:T(8,128)(2,1)} %bitcast.78), calls=%async_computation.3 | async-start | bytes 1572864 | tf_op jit(solution)/shard_map/all_to_all | solution.py:103
  152.4 92.7 %reduce-scatter.5.cloned.1.call-start = ((), (), s32[]{:S(2)}) async-start(), calls=%async_computation.8 | async-start | bytes 1179648 | tf_op jit(solution)/shard_map/reduce_scatter | solution.py:122
  153.3 3.9 %copy-start.10 = (f32[128,256]{1,0:T(8,128)}, f32[128,256]{1,0:T(8,128)S(1)}, u32[]{:S(2)}) copy-start(f32[128,256]{1,0:T(8,128)S(1)} %convert_multiply_fusion.1) | copy-start | bytes 393220
  153.3 26.2 %collective-permute-start = (f32[2,256]{1,0:T(2,128)S(1)}, f32[2,256]{1,0:T(2,128)S(1)}, u32[]{:S(2)}, u32[]{:S(2)}) collective-permute-start(f32[2,256]{1,0:T(2,128)S(1)} %slice.49), channel_id=1, source_target_pairs={{0,4},{4,8},{8,12},{12,16},{16,20},{20,24},{24,28},{1,5},{5,9},{9,... | collective-permute-start | bytes 6152 | tf_op jit(solution)/shard_map/ppermute | solution.py:10
  172.4 7.1 %copy-start.4 = (bf16[2048,256]{1,0:T(8,128)(2,1)S(1)}, bf16[2048,256]{1,0:T(8,128)(2,1)}, u32[]{:S(2)}) copy-start(bf16[2048,256]{1,0:T(8,128)(2,1)} %param.23) | copy-start | bytes 3145732
  172.4 7.1 %copy-start.11 = (f32[128,256]{1,0:T(8,128)S(1)}, f32[128,256]{1,0:T(8,128)}, u32[]{:S(2)}) copy-start(f32[128,256]{1,0:T(8,128)} %copy-done.10) | copy-start | bytes 393220
  172.4 7.1 %copy-start.12 = (bf16[128,256]{1,0:T(8,128)(2,1)S(1)}, bf16[128,256]{1,0:T(8,128)(2,1)}, u32[]{:S(2)}) copy-start(bf16[128,256]{1,0:T(8,128)(2,1)} %param.19) | copy-start | bytes 196612
  180.5 1.5 copy-start.8
  182.0 5.2 %copy-start.19 = (bf16[8,96,2048]{2,1,0:T(8,128)(2,1)S(1)}, bf16[8,96,2048]{2,1,0:T(8,128)(2,1)}, u32[]{:S(2)}) copy-start(bf16[8,96,2048]{2,1,0:T(8,128)(2,1)} %all-gather.5.cloned.1.call-done) | copy-start | bytes 9437188
  182.0 5.2 %copy-start.20 = (f32[768,512]{1,0:T(8,128)S(1)}, f32[768,512]{1,0:T(8,128)}, u32[]{:S(2)}) copy-start(f32[768,512]{1,0:T(8,128)} %fusion.5) | copy-start | bytes 4718596
  182.1 5.2 %copy-start.21 = (f32[768,512]{1,0:T(8,128)S(1)}, f32[768,512]{1,0:T(8,128)}, u32[]{:S(2)}) copy-start(f32[768,512]{1,0:T(8,128)} %fusion.8) | copy-start | bytes 4718596
  187.3 3.3 %copy-start.9 = (f32[128,256]{1,0:T(8,128)S(1)}, f32[128,256]{1,0:T(8,128)}, u32[]{:S(2)}) copy-start(f32[128,256]{1,0:T(8,128)} %get-tuple-element.13) | copy-start | bytes 393220
  187.3 4.8 %copy-start.6 = (bf16[768,512]{1,0:T(8,128)(2,1)S(1)}, bf16[768,512]{1,0:T(8,128)(2,1)}, u32[]{:S(2)}) copy-start(bf16[768,512]{1,0:T(8,128)(2,1)} %copy-done.5) | copy-start | bytes 2359300
  187.3 4.8 %copy-start.18 = (bf16[8,96,2048]{2,1,0:T(8,128)(2,1)S(1)}, bf16[8,96,2048]{2,1,0:T(8,128)(2,1)}, u32[]{:S(2)}) copy-start(bf16[8,96,2048]{2,1,0:T(8,128)(2,1)} %all-gather.3.cloned.1.call-done) | copy-start | bytes 9437188
  190.6 5.6 %copy-start.13 = (bf16[128,256]{1,0:T(8,128)(2,1)S(1)}, bf16[128,256]{1,0:T(8,128)(2,1)}, u32[]{:S(2)}) copy-start(bf16[128,256]{1,0:T(8,128)(2,1)} %param.20) | copy-start | bytes 196612
  190.6 6.3 %copy-start.14 = (bf16[128,256]{1,0:T(8,128)(2,1)S(1)}, bf16[128,256]{1,0:T(8,128)(2,1)}, u32[]{:S(2)}) copy-start(bf16[128,256]{1,0:T(8,128)(2,1)} %param.21) | copy-start | bytes 196612
  190.6 5.6 %collective-permute-start.1 = (f32[2,256]{1,0:T(2,128)S(1)}, f32[2,256]{1,0:T(2,128)S(1)}, u32[]{:S(2)}, u32[]{:S(2)}) collective-permute-start(f32[2,256]{1,0:T(2,128)S(1)} %slice.54), channel_id=1, source_target_pairs={{4,0},{8,4},{12,8},{16,12},{20,16},{24,20},{28,24},{5,1},{9,5},{13... | collective-permute-start | bytes 6152 | tf_op jit(solution)/shard_map/ppermute | solution.py:10
Sparse Core Ops, SparseCore 0:
  39.9 27.5 all-gather.2
  69.0 28.4 all-gather.4
  109.1 37.7 reduce-scatter.2
  182.1 62.8 reduce-scatter.4
where the time goes:
time: 254 us; the launch traced here: 253 us
  waiting for transfers between devices  127 us (50%)
  blocking collectives  57.3 us (23%)
  matrix products  34.8 us (14%)
  between operations  14.1 us (6%)
  starting transfers between devices  11 us (4%)
  other arithmetic  6.23 us (2%)
    reduce_scatter x1, waiting for transfers between devices, per_device(): lax.psum_scatter(lax.dot_general(stream_grad, conv_out, contract_first, p...  47.4 us
    reduce_scatter x1, waiting for transfers between devices, per_device(): lax.psum_scatter(row_partial.astype(jnp.bfloat16), 'tp', scatter_dimensio...  37.9 us
    all_to_all x1, blocking collectives, per_device(): lax.all_to_all(sent_rows, 'sp', split_axis=0, concat_axis=0, tiled=True)  27.3 us
    all_to_all x1, blocking collectives, per_device(): lax.all_to_all(sent_cot, 'sp', split_axis=0, concat_axis=0, tiled=True)  23.3 us
    all_gather x1, waiting for transfers between devices, per_device(): lax.all_gather(recv_cot, 'tp', axis=2, tiled=True)  22.2 us
    all_to_all x1, waiting for transfers between devices, per_device(): lax.all_to_all(half_grad, 'sp', split_axis=0, concat_axis=0, tiled=True)  15.2 us
    all_gather x1, blocking collectives, per_device(): moe_grad = lax.all_gather(moe_part, 'tp', axis=1, tiled=True)  6.68 us
    dot_general x1, matrix products, per_device(): lax.dot_general(routed_cot, down_local, contract_last, preferred_element_...  5.69 us
  transfers between devices with their start and end apart: 7, of which 6 were waited for; matrix products, arithmetic and copies ran while one was open for 9% of the time, Pallas kernels for 0%

commit v1 on v0

--- a/solution.py
+++ b/solution.py
@@ -1,6 +1,10 @@
+import functools
+
 import jax
 import jax.numpy as jnp
 from jax import lax
+from jax.experimental import pallas as pl
+from jax.experimental.pallas import tpu as pltpu
 from jax.sharding import PartitionSpec as P
 
 
@@ -8,6 +12,395 @@
     devices = range(lax.axis_size(axis))
     route = [(i - distance, i) for i in devices if i - distance in devices]
     return lax.ppermute(block, axis, route)
+
+
+def near_first(count):
+    return sorted(range(count), key=lambda d: (min(d, count - d), d))
+
+
+class Seat:
+    def __init__(self, experts, pairs):
+        self.sp = lax.axis_index("sp")
+        self.tp = lax.axis_index("tp")
+        self.half = lax.rem(self.sp, 2)
+        self.expert = self.sp // 2
+        self.core = lax.rem(self.tp, 2)
+        self.row = self.tp // 2
+        self.experts = experts
+        self.pairs = pairs
+
+    def ahead(self, distance):
+        return lax.rem(self.expert + distance, self.experts)
+
+    def behind(self, distance):
+        return lax.rem(self.expert + self.experts - distance, self.experts)
+
+    def other_expert(self, expert):
+        return (expert * 2 + self.half, self.tp)
+
+    def other_half(self):
+        return (self.expert * 2 + 1 - self.half, self.tp)
+
+    def row_ahead(self, distance):
+        return lax.rem(self.row + distance, self.pairs)
+
+    def row_behind(self, distance):
+        return lax.rem(self.row + self.pairs - distance, self.pairs)
+
+    def other_row(self, row):
+        return (self.sp, row * 2 + self.core)
+
+    def other_core(self):
+        return (self.sp, self.row * 2 + 1 - self.core)
+
+
+def remote(src, dst, sent, landed, device):
+    return pltpu.make_async_remote_copy(
+        src_ref=src,
+        dst_ref=dst,
+        send_sem=sent,
+        recv_sem=landed,
+        device_id=device,
+        device_id_type=pl.DeviceIdType.MESH,
+    )
+
+
+def greet(peers):
+    barrier = pltpu.get_barrier_semaphore()
+    for peer in peers:
+        pl.semaphore_signal(barrier, inc=1, device_id=peer, device_id_type=pl.DeviceIdType.MESH)
+    pl.semaphore_wait(barrier, len(peers))
+
+
+def dispatch_kernel(experts, pairs, send_ref, rows_ref, cot_ref,
+                    zs, zr, xs, xr, ys, yr, ds, dr, cs, cr, own):
+    seat = Seat(experts, pairs)
+    width = send_ref.shape[3]
+    offs = near_first(experts)
+    outs = (rows_ref, cot_ref)
+    greet(
+        [seat.other_expert(seat.ahead(d)) for d in range(1, experts)]
+        + [seat.other_half(), seat.other_core()]
+        + [seat.other_row(seat.row_ahead(d)) for d in range(1, pairs)]
+    )
+    started = []
+
+    def place(kind, half, expert, tp):
+        cols = pl.ds(pl.multiple_of(tp * width, width), width)
+        return outs[kind].at[half, expert, :, cols]
+
+    def push(src, dst, sent, landed, device):
+        copy = remote(src, dst, sent, landed, device)
+        copy.start()
+        started.append(copy)
+
+    def landed(spot, sem_s, sem_r):
+        remote(spot, spot, sem_s, sem_r, seat.other_core()).wait_recv()
+
+    items = [(kind, k) for kind in range(2) for k in range(experts)]
+    local = []
+    for kind in range(2):
+        spot = place(kind, seat.half, seat.expert, seat.tp)
+        copy = pltpu.make_async_copy(send_ref.at[kind, seat.expert], spot, own.at[kind])
+        copy.start()
+        local.append(copy)
+        for k in range(1, experts):
+            target = seat.behind(offs[k])
+            push(send_ref.at[kind, target], spot, zs.at[kind, k], zr.at[kind, k],
+                 seat.other_expert(target))
+
+    def first(kind, k):
+        spot = place(kind, seat.half, seat.ahead(offs[k]), seat.tp)
+        if k == 0:
+            src = send_ref.at[kind, seat.expert]
+        else:
+            landed(spot, zs.at[kind, k], zr.at[kind, k])
+            src = spot
+        push(src, spot, xs.at[kind, k], xr.at[kind, k], seat.other_half())
+        for d in range(1, pairs):
+            push(src, spot, ys.at[kind, k, d], yr.at[kind, k, d],
+                 seat.other_row(seat.row_behind(d)))
+        push(src, spot, cs.at[kind, k, 0], cr.at[kind, k, 0], seat.other_core())
+
+    def second(kind, k):
+        expert = seat.ahead(offs[k])
+        spot = place(kind, 1 - seat.half, expert, seat.tp)
+        landed(spot, xs.at[kind, k], xr.at[kind, k])
+        if k % 2 == 0:
+            for d in range(1, pairs):
+                push(spot, spot, ds.at[kind, k, d], dr.at[kind, k, d],
+                     seat.other_row(seat.row_behind(d)))
+        push(spot, spot, cs.at[kind, k, 1], cr.at[kind, k, 1], seat.other_core())
+        for d in range(1, pairs):
+            spot = place(kind, seat.half, expert, seat.row_ahead(d) * 2 + seat.core)
+            landed(spot, ys.at[kind, k, d], yr.at[kind, k, d])
+            if k % 2 == 1:
+                push(spot, spot, ds.at[kind, k, d], dr.at[kind, k, d], seat.other_half())
+            push(spot, spot, cs.at[kind, k, 2 * d], cr.at[kind, k, 2 * d], seat.other_core())
+
+    def third(kind, k):
+        for d in range(1, pairs):
+            spot = place(kind, 1 - seat.half, seat.ahead(offs[k]),
+                         seat.row_ahead(d) * 2 + seat.core)
+            landed(spot, ds.at[kind, k, d], dr.at[kind, k, d])
+            push(spot, spot, cs.at[kind, k, 2 * d + 1], cr.at[kind, k, 2 * d + 1],
+                 seat.other_core())
+
+    for n in range(len(items) + 2):
+        if n < len(items):
+            first(*items[n])
+        if 1 <= n <= len(items):
+            second(*items[n - 1])
+        if n >= 2:
+            third(*items[n - 2])
+    for kind, k in items:
+        expert = seat.ahead(offs[k])
+        for d in range(pairs):
+            tp = seat.row_ahead(d) * 2 + 1 - seat.core
+            for swap in range(2):
+                half = seat.half if swap == 0 else 1 - seat.half
+                landed(place(kind, half, expert, tp),
+                       cs.at[kind, k, 2 * d + swap], cr.at[kind, k, 2 * d + swap])
+    for copy in started:
+        copy.wait_send()
+    for copy in local:
+        copy.wait()
+
+
+def return_kernel(experts, pairs, part_ref, sel_ref, cot_ref, conv_ref, sg_ref, g_ref, c_ref,
+                  a_ref, acc_ref, b1_ref, acc2_ref, b2_ref, fin_ref, ret_ref,
+                  as_, ar, b1s, b1r, b2s, b2r, zs, zr, ms, mr, gs, gr, vs, vr, us, ur, own):
+    seat = Seat(experts, pairs)
+    capacity = part_ref.shape[2]
+    width = part_ref.shape[3] // (2 * pairs)
+    slice_width = g_ref.shape[3]
+    offs = near_first(experts)
+    order = list(reversed(range(experts)))
+    sp_peers = [
+        (expert * 2 + half, seat.tp)
+        for d in range(experts)
+        for expert in [seat.ahead(d)]
+        for half in ([seat.half, 1 - seat.half] if d else [1 - seat.half])
+    ]
+    greet(
+        sp_peers + [seat.other_core()]
+        + [seat.other_row(seat.row_ahead(d)) for d in range(1, pairs)]
+    )
+    started = []
+
+    def cols(tp):
+        return pl.ds(pl.multiple_of(tp * width, width), width)
+
+    def push(src, dst, sent, landed, device):
+        copy = remote(src, dst, sent, landed, device)
+        copy.start()
+        started.append(copy)
+
+    def landed(spot, sem_s, sem_r):
+        remote(spot, spot, sem_s, sem_r, seat.other_core()).wait_recv()
+
+    def total(*terms):
+        value = terms[0].astype(jnp.float32)
+        for term in terms[1:]:
+            value = value + term.astype(jnp.float32)
+        return value.astype(jnp.bfloat16)
+
+    def zone(k):
+        return seat.behind(offs[k])
+
+    for k in order:
+        for half in range(2):
+            for row in range(pairs):
+                push(part_ref.at[half, zone(k), :, cols(row * 2 + 1 - seat.core)],
+                     a_ref.at[half, row, k], as_.at[half, row, k], ar.at[half, row, k],
+                     seat.other_core())
+    copy_conv = pltpu.make_async_copy(conv_ref, c_ref.at[seat.half, seat.expert], own.at[0])
+    copy_conv.start()
+    for k in range(1, experts):
+        push(conv_ref, c_ref.at[seat.half, seat.expert], vs.at[k], vr.at[k],
+             seat.other_expert(seat.behind(offs[k])))
+
+    def first(k):
+        for half in range(2):
+            for row in range(pairs):
+                landed(a_ref.at[half, row, k], as_.at[half, row, k], ar.at[half, row, k])
+                acc_ref[half, row, k] = total(
+                    part_ref[half, zone(k), :, cols(row * 2 + seat.core)], a_ref[half, row, k]
+                )
+        if k % 2 == 0:
+            for row in range(pairs):
+                push(acc_ref.at[1 - seat.half, row, k], b1_ref.at[k, row],
+                     b1s.at[k, row], b1r.at[k, row], seat.other_half())
+        else:
+            for d in range(1, pairs):
+                target = seat.row_behind(d)
+                for half in range(2):
+                    slot = 2 * (d - 1) + half
+                    push(acc_ref.at[half, target, k], b1_ref.at[k, slot],
+                         b1s.at[k, slot], b1r.at[k, slot], seat.other_row(target))
+
+    def second(k):
+        if k % 2 == 0:
+            for row in range(pairs):
+                landed(b1_ref.at[k, row], b1s.at[k, row], b1r.at[k, row])
+                acc2_ref[k, row] = total(acc_ref[seat.half, row, k], b1_ref[k, row])
+            for d in range(1, pairs):
+                target = seat.row_behind(d)
+                push(acc2_ref.at[k, target], b2_ref.at[k, d - 1], b2s.at[k, d - 1],
+                     b2r.at[k, d - 1], seat.other_row(target))
+        else:
+            for half in range(2):
+                terms = [acc_ref[half, seat.row, k]]
+                for d in range(1, pairs):
+                    slot = 2 * (d - 1) + half
+                    landed(b1_ref.at[k, slot], b1s.at[k, slot], b1r.at[k, slot])
+                    terms.append(b1_ref[k, slot])
+                acc2_ref[k, half] = total(*terms)
+            push(acc2_ref.at[k, 1 - seat.half], b2_ref.at[k, 0], b2s.at[k, 0], b2r.at[k, 0],
+                 seat.other_half())
+
+    def third(k):
+        count = pairs - 1 if k % 2 == 0 else 1
+        terms = [acc2_ref[k, seat.row if k % 2 == 0 else seat.half]]
+        for slot in range(count):
+            landed(b2_ref.at[k, slot], b2s.at[k, slot], b2r.at[k, slot])
+            terms.append(b2_ref[k, slot])
+        rows = pl.ds(pl.multiple_of(seat.expert * capacity, 16), capacity)
+        if k == 0:
+            ret_ref[rows, :] = total(*terms)
+        else:
+            fin_ref[k] = total(*terms)
+            push(fin_ref.at[k], ret_ref.at[rows, :], zs.at[k], zr.at[k],
+                 seat.other_expert(zone(k)))
+
+    for n in range(experts + 2):
+        if n < experts:
+            first(order[n])
+        if 1 <= n <= experts:
+            second(order[n - 1])
+        if n >= 2:
+            third(order[n - 2])
+    copy_conv.wait()
+    for k in range(experts):
+        expert = seat.ahead(offs[k])
+        spot = c_ref.at[seat.half, expert]
+        if k:
+            landed(spot, vs.at[k], vr.at[k])
+        push(spot, spot, us.at[k], ur.at[k], seat.other_half())
+    for k in range(1, experts):
+        rows = pl.ds(pl.multiple_of(seat.ahead(offs[k]) * capacity, 16), capacity)
+        landed(ret_ref.at[rows, :], zs.at[k], zr.at[k])
+    moe = jnp.dot(sel_ref[...], ret_ref[...], preferred_element_type=jnp.float32)
+    mine = cols(seat.tp)
+    sg_ref[:, mine] = total(cot_ref[:, mine], moe.astype(jnp.bfloat16))
+    for d in range(1, pairs):
+        push(sg_ref.at[:, mine], sg_ref.at[:, mine], ms.at[2 * d], mr.at[2 * d],
+             seat.other_row(seat.row_behind(d)))
+    push(sg_ref.at[:, mine], sg_ref.at[:, mine], ms.at[0], mr.at[0], seat.other_core())
+    for d in range(1, pairs):
+        theirs = sg_ref.at[:, cols(seat.row_ahead(d) * 2 + seat.core)]
+        landed(theirs, ms.at[2 * d], mr.at[2 * d])
+        push(theirs, theirs, ms.at[2 * d + 1], mr.at[2 * d + 1], seat.other_core())
+    for d in range(pairs):
+        slot = 0 if d == 0 else 2 * d + 1
+        theirs = sg_ref.at[:, cols(seat.row_ahead(d) * 2 + 1 - seat.core)]
+        landed(theirs, ms.at[slot], mr.at[slot])
+
+    def piece(sp):
+        return sg_ref.at[:, pl.ds(pl.multiple_of(sp * slice_width, 128), slice_width)]
+
+    for k in range(experts):
+        expert = seat.behind(offs[k])
+        for swap in range(2):
+            if k == 0 and swap == 0:
+                continue
+            half = seat.half if swap == 0 else 1 - seat.half
+            push(piece(expert * 2 + half), g_ref.at[seat.half, seat.expert],
+                 gs.at[k, swap], gr.at[k, swap], (expert * 2 + half, seat.tp))
+    keep = pltpu.make_async_copy(piece(seat.sp), g_ref.at[seat.half, seat.expert], own.at[1])
+    keep.start()
+    for k in range(experts):
+        expert = seat.ahead(offs[k])
+        landed(c_ref.at[1 - seat.half, expert], us.at[k], ur.at[k])
+        for swap in range(2):
+            if k == 0 and swap == 0:
+                continue
+            half = seat.half if swap == 0 else 1 - seat.half
+            landed(g_ref.at[half, expert], gs.at[k, swap], gr.at[k, swap])
+    for copy in started:
+        copy.wait_send()
+    keep.wait()
+
+
+def vmem(count):
+    return [pl.BlockSpec(memory_space=pltpu.VMEM)] * count
+
+
+def sems(*shape):
+    return pltpu.SemaphoreType.DMA(shape)
+
+
+def dispatch(sent, experts, tp_count):
+    pairs = tp_count // 2
+    _, _, capacity, width = sent.shape
+    shape = jax.ShapeDtypeStruct((2, experts, capacity, width * tp_count), jnp.bfloat16)
+    flat, rowed = (2, experts), (2, experts, pairs)
+    cored = (2, experts, 2 * pairs)
+    return pl.pallas_call(
+        functools.partial(dispatch_kernel, experts, pairs),
+        out_shape=(shape, shape),
+        in_specs=vmem(1),
+        out_specs=tuple(vmem(2)),
+        scratch_shapes=[
+            sems(*s)
+            for s in (flat, flat, flat, flat, rowed, rowed, rowed, rowed, cored, cored, (2,))
+        ],
+        compiler_params=pltpu.CompilerParams(
+            collective_id=0, has_side_effects=True, vmem_limit_bytes=32 * 1024 * 1024
+        ),
+    )(sent)
+
+
+def give_back(part, select_t, cotangent, conv_out, experts, tp_count):
+    pairs = tp_count // 2
+    _, _, capacity, model_width = part.shape
+    tokens, channels = conv_out.shape
+    width = model_width // tp_count
+    groups = 2 * experts
+    most = max(pairs, 2 * (pairs - 1))
+    late = max(pairs - 1, 1)
+    bf16 = jnp.bfloat16
+    return pl.pallas_call(
+        functools.partial(return_kernel, experts, pairs),
+        out_shape=(
+            jax.ShapeDtypeStruct((tokens, model_width), bf16),
+            jax.ShapeDtypeStruct((2, experts, tokens, model_width // groups), bf16),
+            jax.ShapeDtypeStruct((2, experts, tokens, channels), bf16),
+        ),
+        in_specs=vmem(4),
+        out_specs=tuple(vmem(3)),
+        scratch_shapes=[
+            pltpu.VMEM((2, pairs, experts, capacity, width), bf16),
+            pltpu.VMEM((2, pairs, experts, capacity, width), bf16),
+            pltpu.VMEM((experts, most, capacity, width), bf16),
+            pltpu.VMEM((experts, max(pairs, 2), capacity, width), bf16),
+            pltpu.VMEM((experts, late, capacity, width), bf16),
+            pltpu.VMEM((experts, capacity, width), bf16),
+            pltpu.VMEM((experts * capacity, width), bf16),
+        ]
+        + [
+            sems(*s)
+            for shape in (
+                (2, pairs, experts), (experts, most), (experts, late), (experts,),
+                (2 * pairs,), (experts, 2), (experts,), (experts,),
+            )
+            for s in (shape, shape)
+        ]
+        + [sems(2)],
+        compiler_params=pltpu.CompilerParams(
+            collective_id=1, has_side_effects=True, vmem_limit_bytes=40 * 1024 * 1024
+        ),
+    )(part, select_t, cotangent, conv_out)
 
 
 def per_device(
@@ -52,19 +445,26 @@
     sent_cot = (
         jnp.dot(select, cot_part, preferred_element_type=jnp.float32) * slot_weight[:, None]
     ).astype(jnp.bfloat16)
-    sent_rows = jnp.repeat(sent_rows.reshape(experts, capacity, -1), 2, axis=0)
-    sent_cot = jnp.repeat(sent_cot.reshape(experts, capacity, -1), 2, axis=0)
-    recv_rows, recv_cot = (
-        lax.all_to_all(sent_rows, "sp", split_axis=0, concat_axis=0, tiled=True),
-        lax.all_to_all(sent_cot, "sp", split_axis=0, concat_axis=0, tiled=True),
-    )
-    recv_rows, recv_cot = (
-        lax.all_gather(recv_rows, "tp", axis=2, tiled=True),
-        lax.all_gather(recv_cot, "tp", axis=2, tiled=True),
-    )
+    direct = tp_count % 2 == 0 and capacity % 16 == 0 and block_width % 128 == 0
     slots = groups * capacity
-    routed_rows = recv_rows.reshape(slots, model_width)
-    routed_cot = recv_cot.reshape(slots, model_width)
+    if direct:
+        sent = jnp.stack([sent_rows, sent_cot]).reshape(2, experts, capacity, block_width)
+        routed_rows, routed_cot = dispatch(sent, experts, tp_count)
+        routed_rows = routed_rows.reshape(slots, model_width)
+        routed_cot = routed_cot.reshape(slots, model_width)
+    else:
+        sent_rows = jnp.repeat(sent_rows.reshape(experts, capacity, -1), 2, axis=0)
+        sent_cot = jnp.repeat(sent_cot.reshape(experts, capacity, -1), 2, axis=0)
+        recv_rows, recv_cot = (
+            lax.all_to_all(sent_rows, "sp", split_axis=0, concat_axis=0, tiled=True),
+            lax.all_to_all(sent_cot, "sp", split_axis=0, concat_axis=0, tiled=True),
+        )
+        recv_rows, recv_cot = (
+            lax.all_gather(recv_rows, "tp", axis=2, tiled=True),
+            lax.all_gather(recv_cot, "tp", axis=2, tiled=True),
+        )
+        routed_rows = recv_rows.reshape(slots, model_width)
+        routed_cot = recv_cot.reshape(slots, model_width)
     gate_local = gate_weight[0]
     up_local = up_weight[0]
     down_local = down_weight[0]
@@ -95,21 +495,6 @@
     row_partial = row_partial + lax.dot_general(
         up_delta, up_local, contract_last, preferred_element_type=jnp.float32
     )
-    half_sums = lax.psum_scatter(
-        row_partial.astype(jnp.bfloat16), "tp", scatter_dimension=1, tiled=True
-    ).astype(jnp.float32)
-    block_width = half_sums.shape[1]
-    half_grad = half_sums.reshape(groups, capacity, block_width).astype(jnp.bfloat16)
-    returned = lax.all_to_all(half_grad, "sp", split_axis=0, concat_axis=0, tiled=True)
-    returned = returned.reshape(experts, 2, capacity, block_width)
-    select_three = select.reshape(experts, capacity, tok_rows)
-    moe_part = jnp.einsum(
-        "ecr,emcd->rd", select_three, returned, preferred_element_type=jnp.float32
-    ).astype(jnp.bfloat16)
-    moe_grad = lax.all_gather(moe_part, "tp", axis=1, tiled=True)
-    stream_grad = (cotangent.astype(jnp.float32) + moe_grad.astype(jnp.float32)).astype(
-        jnp.bfloat16
-    )
     taps = conv_taps.astype(jnp.float32)
     outer_f = outer_gate.astype(jnp.float32)
     inner_f = inner_gate.astype(jnp.float32)
@@ -119,14 +504,45 @@
     padded = jnp.concatenate([earlier, mixed], axis=0)
     conv_sum = taps[0] * padded[:-2] + taps[1] * padded[1:-1] + taps[2] * padded[2:]
     conv_out = (outer_f * conv_sum).astype(jnp.bfloat16)
-    out_grad = lax.psum_scatter(
-        lax.dot_general(
-            stream_grad, conv_out, contract_first, preferred_element_type=jnp.float32
-        ).astype(jnp.bfloat16),
-        "sp",
-        scatter_dimension=0,
-        tiled=True,
-    ).astype(jnp.float32)
+    if direct:
+        stream_grad, grad_all, conv_all = give_back(
+            row_partial.astype(jnp.bfloat16).reshape(2, experts, capacity, model_width),
+            select.T,
+            cotangent,
+            conv_out,
+            experts,
+            tp_count,
+        )
+        out_grad = lax.dot_general(
+            grad_all.reshape(groups * tok_rows, -1),
+            conv_all.reshape(groups * tok_rows, -1),
+            contract_first,
+            preferred_element_type=jnp.float32,
+        )
+    else:
+        half_sums = lax.psum_scatter(
+            row_partial.astype(jnp.bfloat16), "tp", scatter_dimension=1, tiled=True
+        ).astype(jnp.float32)
+        block_width = half_sums.shape[1]
+        half_grad = half_sums.reshape(groups, capacity, block_width).astype(jnp.bfloat16)
+        returned = lax.all_to_all(half_grad, "sp", split_axis=0, concat_axis=0, tiled=True)
+        returned = returned.reshape(experts, 2, capacity, block_width)
+        select_three = select.reshape(experts, capacity, tok_rows)
+        moe_part = jnp.einsum(
+            "ecr,emcd->rd", select_three, returned, preferred_element_type=jnp.float32
+        ).astype(jnp.bfloat16)
+        moe_grad = lax.all_gather(moe_part, "tp", axis=1, tiled=True)
+        stream_grad = (cotangent.astype(jnp.float32) + moe_grad.astype(jnp.float32)).astype(
+            jnp.bfloat16
+        )
+        out_grad = lax.psum_scatter(
+            lax.dot_general(
+                stream_grad, conv_out, contract_first, preferred_element_type=jnp.float32
+            ).astype(jnp.bfloat16),
+            "sp",
+            scatter_dimension=0,
+            tiled=True,
+        ).astype(jnp.float32)
     conv_grad = jnp.dot(stream_grad, out_weight, preferred_element_type=jnp.float32)
     outer_grad = (conv_grad * conv_sum).astype(jnp.bfloat16)
     scaled = conv_grad * outer_f

time: 254 us -> 126 us (0.50)
  waiting for transfers between devices: 127 us -> 3.14 us
  Pallas kernels: 0 us -> 84.6 us
  blocking collectives: 57.3 us -> 0 us
  between operations: 14.1 us -> 0.9 us
  matrix products: 34.8 us -> 23.6 us
  starting transfers between devices: 11 us -> 6.15 us
    reduce_scatter x2 -> x0, waiting for transfers between devices: 85.3 us -> none  [the longest x1 47.4 us: per_device(): lax.psum_scatter(lax.dot_general(stream_grad, conv_out, contract_first, p...]
    pallas_call x0 -> x2, Pallas kernels: none -> 84.6 us  [the longest x1 45.1 us: give_back(): pl.pallas_call(functools.partial(return_kernel, experts, pairs), out_shap...]
    all_to_all x2 -> x0, blocking collectives: 50.6 us -> none  [the longest x1 27.3 us: per_device(): lax.all_to_all(sent_rows, 'sp', split_axis=0, concat_axis=0, tiled=True)]
    all_gather x2 -> x0, waiting for transfers between devices: 25.7 us -> none  [the longest x1 22.2 us: per_device(): lax.all_gather(recv_cot, 'tp', axis=2, tiled=True)]
    all_to_all x1 -> x0, waiting for transfers between devices: 15.2 us -> none  [per_device(): lax.all_to_all(half_grad, 'sp', split_axis=0, concat_axis=0, tiled=True)]
    all_gather x1 -> x0, blocking collectives: 6.68 us -> none  [per_device(): moe_grad = lax.all_gather(moe_part, 'tp', axis=1, tiled=True)]
    all_to_all x1 -> x0, starting transfers between devices: 5.51 us -> none  [per_device(): lax.all_to_all(half_grad, 'sp', split_axis=0, concat_axis=0, tiled=True)]
    dot_general x1, matrix products: 5.69 us -> 2.27 us  [per_device(): lax.dot_general(routed_cot, down_local, contract_last, preferred_element_...]
  transfers between devices with their start and end apart: 7 -> 2, of which waited for: 6 -> 1; matrix products, arithmetic and copies ran while one was open for 9% -> 22% of each run, Pallas kernels for 0% -> 31%
where the time goes in v1:
time: 126 us
  Pallas kernels  84.6 us (67%)
  matrix products  23.6 us (19%)
  starting transfers between devices  6.15 us (5%)
  other arithmetic  4.78 us (4%)
  waiting for transfers between devices  3.14 us (2%)
  local copies, waits for them, and re-layouts  2.65 us (2%)
    pallas_call x1, Pallas kernels, give_back(): pl.pallas_call(functools.partial(return_kernel, experts, pairs), out_shap...  45.1 us
    pallas_call x1, Pallas kernels, dispatch(): pl.pallas_call(functools.partial(dispatch_kernel, experts, pairs), out_sh...  39.5 us
    ppermute x2, starting transfers between devices, from_behind(): return lax.ppermute(block, axis, route)  6.15 us
    dot_general x1, matrix products, per_device(): lax.dot_general(hidden, routed_cot, contract_first, preferred_element_typ...  3.25 us
    dot_general x1, matrix products, per_device(): lax.dot_general(routed_rows, gate_delta, contract_first, preferred_elemen...  3.16 us
    dot_general x1, matrix products, per_device(): lax.dot_general(routed_rows, up_delta, contract_first, preferred_element_...  3.16 us
    ppermute x2, waiting for transfers between devices, from_behind(): return lax.ppermute(block, axis, route)  3.14 us
  transfers between devices with their start and end apart: 2, of which 1 were waited for; matrix products, arithmetic and copies ran while one was open for 22% of the time, Pallas kernels for 31%

profile of v1, /device:TPU:0, one launch (start us, length us, event | category | flops | bytes accessed | tf_op | source)
XLA Modules:
  0.0 125.9 jit_solution(17179250185801217608)
XLA Ops:
  0.6 0.0 copy-start
  0.6 1.0 convert_multiply_fusion.1
  1.7 4.9 %collective-permute-start = (f32[2,256]{1,0:T(2,128)S(1)}, f32[2,256]{1,0:T(2,128)S(1)}, u32[]{:S(2)}, u32[]{:S(2)}) collective-permute-start(f32[2,256]{1,0:T(2,128)S(1)} %slice.49), channel_id=1, source_target_pairs={{0,4},{4,8},{8,12},{12,16},{16,20},{20,24},{24,28},{1,5},{5,9},{9,... | collective-permute-start | bytes 6152 | tf_op jit(solution)/shard_map/ppermute | solution.py:14
  6.6 0.8 copy.41
  7.4 0.1 eq.50
  7.5 0.1 eq.46
  7.7 1.2 reduce-window.6
  8.9 0.1 slice.47
  9.0 0.1 copy.43
  9.1 0.1 copy.44
  9.2 0.1 add_bitcast_fusion
  9.3 0.1 reduce_sum.30
  9.5 0.8 copy.47
  10.2 0.1 mul.132
  10.4 0.1 copy.45
  10.4 0.7 multiply_add_fusion.1
  11.2 0.1 convert_reduce_fusion
  11.2 0.1 copy.46
  11.3 0.2 select_reduce_fusion
  11.5 1.2 convolution_convert_fusion.3
  12.7 1.2 fusion.13
  13.9 0.1 pad_maximum_fusion.send_ref
  14.0 39.5 %shard_map.171 = (bf16[2,4,96,2048]{3,2,1,0:T(8,128)(2,1)S(1)}, bf16[2,4,96,2048]{3,2,1,0:T(8,128)(2,1)S(1)}) custom-call(bf16[2,4,96,512]{3,2,1,0:T(8,128)(2,1)S(1)} %pad_maximum_fusion.send_ref), custom_call_target="tpu_custom_call" | custom-call | tf_op jit(solution)/shard_map/pallas_call | solution.py:349
  53.5 0.0 copy-start.2
  53.5 1.8 %fusion.5 = f32[768,512]{1,0:T(8,128)S(1)} fusion(bf16[768,2048]{1,0:T(8,128)(2,1)S(1)} %bitcast.73, bf16[1,2048,512]{2,1,0:T(8,128)(2,1)S(1)} %copy-done), kind=kOutput, calls=%fused_computation.9 | convolution fusion | flops 1610612736 | bytes 6815744 | tf_op jit(solution)/shard_map/dot_general | solution.py:471
  55.3 0.0 copy-done.2
  55.3 1.8 %fusion.8 = f32[768,512]{1,0:T(8,128)S(1)} fusion(bf16[768,2048]{1,0:T(8,128)(2,1)S(1)} %bitcast.74, bf16[1,2048,512]{2,1,0:T(8,128)(2,1)S(1)} %copy-done.2), kind=kOutput, calls=%fused_computation.12 | convolution fusion | flops 1610612736 | bytes 6815744 | tf_op jit(solution)/shard_map/dot_general | solution.py:472
  57.1 0.0 copy-start.8
  57.1 3.3 %fusion.2 = bf16[1,512,2048]{2,1,0:T(8,128)(2,1)} fusion(bf16[768,2048]{1,0:T(8,128)(2,1)S(1)} %bitcast.77, f32[768,512]{1,0:T(8,128)S(1)} %fusion.8, f32[768,512]{1,0:T(8,128)S(1)} %fusion.5), kind=kOutput, calls=%fused_computation.6 | convolution fusion | flops 1614020608 | bytes 8388608 | tf_op jit(solution)/shard_map/dot_general | solution.py:489
  60.3 2.3 %multiply_convert_fusion.1 = (bf16[768,512]{1,0:T(8,128)(2,1)S(1)}, bf16[768,512]{1,0:T(8,128)(2,1)S(1)}) fusion(f32[768,512]{1,0:T(8,128)S(1)} %fusion.5, f32[768,512]{1,0:T(8,128)S(1)} %fusion.8, bf16[768,2048]{1,0:T(8,128)(2,1)S(1)} %bitcast.78, bf16[1,512,2048]{2,1,0:T(8,128)(2,1)S(1)} %copy-done.8), kind=kOutput, calls=%fused_computation.17 | convolution fusion | flops 1615724544 | bytes 9961472 | tf_op jit(solution)/shard_map/dot_general | solution.py:473
  62.6 3.2 %fusion = bf16[1,2048,512]{2,1,0:T(8,128)(2,1)} fusion(bf16[768,2048]{1,0:T(8,128)(2,1)S(1)} %bitcast.75, bf16[768,512]{1,0:T(8,128)(2,1)S(1)} %get-tuple-element.22), kind=kOutput, calls=%fused_computation.4 | convolution fusion | flops 1611661312 | bytes 6029312 | tf_op jit(solution)/shard_map/dot_general | solution.py:483
  65.8 1.8 %fusion.3 = f32[768,2048]{1,0:T(8,128)S(1)} fusion(bf16[768,512]{1,0:T(8,128)(2,1)S(1)} %get-tuple-element.22, bf16[1,2048,512]{2,1,0:T(8,128)(2,1)S(1)} %copy-done), kind=kOutput, calls=%fused_computation.7 | convolution fusion | flops 1610612736 | bytes 9175040 | tf_op jit(solution)/shard_map/dot_general | solution.py:492
  67.6 3.2 %fusion.1 = bf16[1,2048,512]{2,1,0:T(8,128)(2,1)} fusion(bf16[768,2048]{1,0:T(8,128)(2,1)S(1)} %bitcast.76, bf16[768,512]{1,0:T(8,128)(2,1)S(1)} %get-tuple-element.21), kind=kOutput, calls=%fused_computation.5 | convolution fusion | flops 1611661312 | bytes 6029312 | tf_op jit(solution)/shard_map/dot_general | solution.py:486
  70.8 2.0 %add_convert_fusion = bf16[768,2048]{1,0:T(8,128)(2,1)S(1)} fusion(f32[768,2048]{1,0:T(8,128)S(1)} %fusion.3, bf16[768,512]{1,0:T(8,128)(2,1)S(1)} %get-tuple-element.21, bf16[1,2048,512]{2,1,0:T(8,128)(2,1)S(1)} %copy-done.2), kind=kOutput, calls=%fused_computation | convolution fusion | flops 1613758464 | bytes 12320768 | tf_op jit(solution)/shard_map/dot_general | solution.py:495
  72.8 0.0 copy-done.7
  72.8 0.0 collective-permute-done
  72.8 0.0 copy-start.3
  72.9 0.1 fusion.23
  72.9 45.1 %shard_map.172 = (bf16[128,2048]{1,0:T(8,128)(2,1)S(1)}, bf16[2,4,128,256]{3,2,1,0:T(8,128)(2,1)S(1)}, bf16[2,4,128,256]{3,2,1,0:T(8,128)(2,1)S(1)}) custom-call(bf16[2,4,96,2048]{3,2,1,0:T(8,128)(2,1)S(1)} %bitcast.71, bf16[128,384]{1,0:T(8,128)(2,1)S(1)} %bitcast.72, bf16[128,2048]{1,0:T(8,128)(2,1)S(1)} %copy-done.1, ...), custom_call_target="tpu_custom_call" | custom-call | tf_op jit(solution)/shard_map/pallas_call | solution.py:373
  118.1 0.0 copy-start.5
  118.1 0.0 copy-start.6
  118.1 0.0 copy-done.3
  118.1 0.9 convert_multiply_fusion.3
  119.0 1.3 %collective-permute-start.1 = (f32[2,256]{1,0:T(2,128)S(1)}, f32[2,256]{1,0:T(2,128)S(1)}, u32[]{:S(2)}, u32[]{:S(2)}) collective-permute-start(f32[2,256]{1,0:T(2,128)S(1)} %slice.54), channel_id=1, source_target_pairs={{4,0},{8,4},{12,8},{16,12},{20,16},{24,20},{28,24},{5,1},{9,5},{13... | collective-permute-start | bytes 6152 | tf_op jit(solution)/shard_map/ppermute | solution.py:14
  120.3 1.0 convolution_bitcast_fusion
  121.4 3.1 %collective-permute-done.1 = f32[2,256]{1,0:T(2,128)S(1)} collective-permute-done((f32[2,256]{1,0:T(2,128)S(1)}, f32[2,256]{1,0:T(2,128)S(1)}, u32[]{:S(2)}, u32[]{:S(2)}) %collective-permute-start.1) | collective-permute-done | bytes 2080 | tf_op jit(solution)/shard_map/ppermute | solution.py:14
  124.5 0.7 fusion.24
  125.2 0.6 fusion.25
  (17 shorter events, 0.1 us)
Async XLA Ops:
  0.6 52.8 %copy-start = (bf16[1,2048,512]{2,1,0:T(8,128)(2,1)S(1)}, bf16[1,2048,512]{2,1,0:T(8,128)(2,1)}, u32[]{:S(2)}) copy-start(bf16[1,2048,512]{2,1,0:T(8,128)(2,1)} %param.16) | copy-start | bytes 6291460
  1.7 71.1 %collective-permute-start = (f32[2,256]{1,0:T(2,128)S(1)}, f32[2,256]{1,0:T(2,128)S(1)}, u32[]{:S(2)}, u32[]{:S(2)}) collective-permute-start(f32[2,256]{1,0:T(2,128)S(1)} %slice.49), channel_id=1, source_target_pairs={{0,4},{4,8},{8,12},{12,16},{16,20},{20,24},{24,28},{1,5},{5,9},{9,... | collective-permute-start | bytes 6152 | tf_op jit(solution)/shard_map/ppermute | solution.py:14
  53.5 1.8 %copy-start.2 = (bf16[1,2048,512]{2,1,0:T(8,128)(2,1)S(1)}, bf16[1,2048,512]{2,1,0:T(8,128)(2,1)}, u32[]{:S(2)}) copy-start(bf16[1,2048,512]{2,1,0:T(8,128)(2,1)} %param.17) | copy-start | bytes 6291460
  57.1 3.3 %copy-start.8 = (bf16[1,512,2048]{2,1,0:T(8,128)(2,1)S(1)}, bf16[1,512,2048]{2,1,0:T(8,128)(2,1)}, u32[]{:S(2)}) copy-start(bf16[1,512,2048]{2,1,0:T(8,128)(2,1)} %param.18) | copy-start | bytes 6291460
  70.8 2.0 %copy-start.7 = (bf16[3,256]{1,0:T(4,128)(2,1)S(1)}, bf16[3,256]{1,0:T(4,128)(2,1)}, u32[]{:S(2)}) copy-start(bf16[3,256]{1,0:T(4,128)(2,1)} %param.22) | copy-start | bytes 4612
  70.8 2.1 %copy-start.4 = (bf16[128,256]{1,0:T(8,128)(2,1)S(1)}, bf16[128,256]{1,0:T(8,128)(2,1)}, u32[]{:S(2)}) copy-start(bf16[128,256]{1,0:T(8,128)(2,1)} %param.19) | copy-start | bytes 196612
  70.8 2.2 %copy-start.1 = (bf16[128,2048]{1,0:T(8,128)(2,1)S(1)}, bf16[128,2048]{1,0:T(8,128)(2,1)}, u32[]{:S(2)}) copy-start(bf16[128,2048]{1,0:T(8,128)(2,1)} %cot_ref.1) | copy-start | bytes 1572868
  72.8 45.2 %copy-start.3 = (bf16[2048,256]{1,0:T(8,128)(2,1)S(1)}, bf16[2048,256]{1,0:T(8,128)(2,1)}, u32[]{:S(2)}) copy-start(bf16[2048,256]{1,0:T(8,128)(2,1)} %param.23) | copy-start | bytes 3145732
  118.1 6.4 %copy-start.5 = (bf16[128,256]{1,0:T(8,128)(2,1)S(1)}, bf16[128,256]{1,0:T(8,128)(2,1)}, u32[]{:S(2)}) copy-start(bf16[128,256]{1,0:T(8,128)(2,1)} %param.20) | copy-start | bytes 196612
  118.1 7.1 %copy-start.6 = (bf16[128,256]{1,0:T(8,128)(2,1)S(1)}, bf16[128,256]{1,0:T(8,128)(2,1)}, u32[]{:S(2)}) copy-start(bf16[128,256]{1,0:T(8,128)(2,1)} %param.21) | copy-start | bytes 196612
  119.0 5.5 %collective-permute-start.1 = (f32[2,256]{1,0:T(2,128)S(1)}, f32[2,256]{1,0:T(2,128)S(1)}, u32[]{:S(2)}, u32[]{:S(2)}) collective-permute-start(f32[2,256]{1,0:T(2,128)S(1)} %slice.54), channel_id=1, source_target_pairs={{4,0},{8,4},{12,8},{16,12},{20,16},{24,20},{28,24},{5,1},{9,5},{13... | collective-permute-start | bytes 6152 | tf_op jit(solution)/shard_map/ppermute | solution.py:14

commit v2 on v1

--- a/solution.py
+++ b/solution.py
@@ -38,6 +38,10 @@
     def other_expert(self, expert):
         return (expert * 2 + self.half, self.tp)
 
+    def next_tokens(self, distance):
+        groups = 2 * self.experts
+        return (lax.rem(self.sp + groups + distance, groups), self.tp)
+
     def other_half(self):
         return (self.expert * 2 + 1 - self.half, self.tp)
 
@@ -69,21 +73,57 @@
     barrier = pltpu.get_barrier_semaphore()
     for peer in peers:
         pl.semaphore_signal(barrier, inc=1, device_id=peer, device_id_type=pl.DeviceIdType.MESH)
-    pl.semaphore_wait(barrier, len(peers))
-
-
-def dispatch_kernel(experts, pairs, send_ref, rows_ref, cot_ref,
-                    zs, zr, xs, xr, ys, yr, ds, dr, cs, cr, own):
+    return lambda: pl.semaphore_wait(barrier, len(peers))
+
+
+def dispatch_kernel(experts, pairs, routes_ref, weights_ref, stream_ref, given_ref, mixed_ref,
+                    rows_ref, cot_ref, select_ref, early_ref, send_ref, tail_ref,
+                    zs, zr, xs, xr, ys, yr, ds, dr, cs, cr, own, hs, hr):
     seat = Seat(experts, pairs)
-    width = send_ref.shape[3]
+    capacity, width = send_ref.shape[2:]
+    tokens = routes_ref.shape[1]
     offs = near_first(experts)
     outs = (rows_ref, cot_ref)
-    greet(
+    all_here = greet(
+        [seat.next_tokens(1), seat.next_tokens(-1)] +
         [seat.other_expert(seat.ahead(d)) for d in range(1, experts)]
         + [seat.other_half(), seat.other_core()]
         + [seat.other_row(seat.row_ahead(d)) for d in range(1, pairs)]
     )
     started = []
+    tail_ref[...] = mixed_ref[tokens - tail_ref.shape[0]:, :]
+    number = lax.broadcasted_iota(jnp.int32, (experts, tokens), 0)
+    named = [routes_ref[k:k + 1, :] == number for k in range(2)]
+    member = jnp.where(named[0] | named[1], 1.0, 0.0)
+    share = jnp.where(named[0], weights_ref[0:1, :], 0.0) + jnp.where(
+        named[1], weights_ref[1:2, :], 0.0
+    )
+    sooner = lax.broadcasted_iota(jnp.int32, (tokens, tokens), 0) < lax.broadcasted_iota(
+        jnp.int32, (tokens, tokens), 1
+    )
+    rank = jnp.dot(
+        member.astype(jnp.bfloat16),
+        jnp.where(sooner, 1.0, 0.0).astype(jnp.bfloat16),
+        preferred_element_type=jnp.float32,
+    )
+    slot = lax.broadcasted_iota(jnp.int32, (capacity, tokens), 0).astype(jnp.float32)
+    mine = pl.ds(pl.multiple_of(seat.tp * width, width), width)
+    slot_weight = []
+    for e in range(experts):
+        chosen = jnp.where(slot == rank[e:e + 1], member[e:e + 1], 0.0)
+        slot_weight.append(jnp.sum(chosen * share[e:e + 1], axis=1, keepdims=True))
+        select_ref[e * capacity:(e + 1) * capacity, :] = chosen.astype(jnp.bfloat16)
+
+    def fill(kind):
+        block = stream_ref[:, mine] if kind == 0 else given_ref[:, mine]
+        for e in range(experts):
+            picked = jnp.dot(
+                select_ref[e * capacity:(e + 1) * capacity, :], block,
+                preferred_element_type=jnp.float32,
+            )
+            if kind:
+                picked = picked * slot_weight[e]
+            send_ref[kind, e] = picked.astype(jnp.bfloat16)
 
     def place(kind, half, expert, tp):
         cols = pl.ds(pl.multiple_of(tp * width, width), width)
@@ -100,6 +140,9 @@
     items = [(kind, k) for kind in range(2) for k in range(experts)]
     local = []
     for kind in range(2):
+        fill(kind)
+        if kind == 0:
+            all_here()
         spot = place(kind, seat.half, seat.expert, seat.tp)
         copy = pltpu.make_async_copy(send_ref.at[kind, seat.expert], spot, own.at[kind])
         copy.start()
@@ -108,6 +151,8 @@
             target = seat.behind(offs[k])
             push(send_ref.at[kind, target], spot, zs.at[kind, k], zr.at[kind, k],
                  seat.other_expert(target))
+
+    push(tail_ref, early_ref, hs.at[0], hr.at[0], seat.next_tokens(1))
 
     def first(kind, k):
         spot = place(kind, seat.half, seat.ahead(offs[k]), seat.tp)
@@ -161,15 +206,18 @@
                 half = seat.half if swap == 0 else 1 - seat.half
                 landed(place(kind, half, expert, tp),
                        cs.at[kind, k, 2 * d + swap], cr.at[kind, k, 2 * d + swap])
+    landed(early_ref, hs.at[0], hr.at[0])
     for copy in started:
         copy.wait_send()
     for copy in local:
         copy.wait()
 
 
-def return_kernel(experts, pairs, part_ref, sel_ref, cot_ref, conv_ref, sg_ref, g_ref, c_ref,
-                  a_ref, acc_ref, b1_ref, acc2_ref, b2_ref, fin_ref, ret_ref,
-                  as_, ar, b1s, b1r, b2s, b2r, zs, zr, ms, mr, gs, gr, vs, vr, us, ur, own):
+def return_kernel(experts, pairs, part_ref, sel_ref, cot_ref, conv_ref, sum_ref, outer_ref,
+                  inner_ref, input_ref, taps_ref, weight_ref,
+                  out_grad_ref, outer_grad_ref, inner_grad_ref, input_grad_ref,
+                  sg_ref, g_ref, c_ref, ext_ref, late_ref, a_ref, acc_ref, b1_ref, acc2_ref, b2_ref, fin_ref, ret_ref,
+                  as_, ar, b1s, b1r, b2s, b2r, zs, zr, ms, mr, gs, gr, vs, vr, us, ur, hs, hr, own):
     seat = Seat(experts, pairs)
     capacity = part_ref.shape[2]
     width = part_ref.shape[3] // (2 * pairs)
@@ -185,7 +233,7 @@
     greet(
         sp_peers + [seat.other_core()]
         + [seat.other_row(seat.row_ahead(d)) for d in range(1, pairs)]
-    )
+    )()
     started = []
 
     def cols(tp):
@@ -290,7 +338,10 @@
     for k in range(1, experts):
         rows = pl.ds(pl.multiple_of(seat.ahead(offs[k]) * capacity, 16), capacity)
         landed(ret_ref.at[rows, :], zs.at[k], zr.at[k])
-    moe = jnp.dot(sel_ref[...], ret_ref[...], preferred_element_type=jnp.float32)
+    over_first = (((0,), (0,)), ((), ()))
+    moe = lax.dot_general(
+        sel_ref[...], ret_ref[...], over_first, preferred_element_type=jnp.float32
+    )
     mine = cols(seat.tp)
     sg_ref[:, mine] = total(cot_ref[:, mine], moe.astype(jnp.bfloat16))
     for d in range(1, pairs):
@@ -319,6 +370,31 @@
                  gs.at[k, swap], gr.at[k, swap], (expert * 2 + half, seat.tp))
     keep = pltpu.make_async_copy(piece(seat.sp), g_ref.at[seat.half, seat.expert], own.at[1])
     keep.start()
+    tokens = sum_ref.shape[0]
+    border = late_ref.shape[0]
+    conv_grad = jnp.dot(sg_ref[...], weight_ref[...], preferred_element_type=jnp.float32)
+    ext_ref[0:tokens, :] = conv_grad * outer_ref[...].astype(jnp.float32)
+    push(ext_ref.at[0:border, :], late_ref, hs.at[0], hr.at[0], seat.next_tokens(-1))
+    outer_grad_ref[...] = (conv_grad * sum_ref[...]).astype(jnp.bfloat16)
+    keep.wait()
+    out_grad_ref[...] = jnp.zeros_like(out_grad_ref)
+
+    def add_out(half, expert):
+        out_grad_ref[...] += lax.dot_general(
+            g_ref[half, expert], c_ref[half, expert], over_first,
+            preferred_element_type=jnp.float32,
+        )
+
+    add_out(seat.half, seat.expert)
+    landed(late_ref, hs.at[0], hr.at[0])
+    ext_ref[tokens:tokens + border, :] = jnp.where(
+        seat.sp == 2 * experts - 1, 0.0, late_ref[...]
+    )
+    mixed_grad = taps_ref[2:3, :] * ext_ref[0:tokens, :]
+    mixed_grad = mixed_grad + taps_ref[1:2, :] * ext_ref[1:tokens + 1, :]
+    mixed_grad = mixed_grad + taps_ref[0:1, :] * ext_ref[2:tokens + 2, :]
+    inner_grad_ref[...] = (mixed_grad * input_ref[...].astype(jnp.float32)).astype(jnp.bfloat16)
+    input_grad_ref[...] = (mixed_grad * inner_ref[...].astype(jnp.float32)).astype(jnp.bfloat16)
     for k in range(experts):
         expert = seat.ahead(offs[k])
         landed(c_ref.at[1 - seat.half, expert], us.at[k], ur.at[k])
@@ -327,9 +403,9 @@
                 continue
             half = seat.half if swap == 0 else 1 - seat.half
             landed(g_ref.at[half, expert], gs.at[k, swap], gr.at[k, swap])
+            add_out(half, expert)
     for copy in started:
         copy.wait_send()
-    keep.wait()
 
 
 def vmem(count):
@@ -340,46 +416,70 @@
     return pltpu.SemaphoreType.DMA(shape)
 
 
-def dispatch(sent, experts, tp_count):
+def dispatch(routes, route_weights, stream, cotangent, mixed, capacity, experts, tp_count):
     pairs = tp_count // 2
-    _, _, capacity, width = sent.shape
-    shape = jax.ShapeDtypeStruct((2, experts, capacity, width * tp_count), jnp.bfloat16)
+    tokens, model_width = stream.shape
+    width = model_width // tp_count
+    border = min(8, tokens)
+    shape = jax.ShapeDtypeStruct((2, experts, capacity, model_width), jnp.bfloat16)
+    halo = (border, mixed.shape[1])
     flat, rowed = (2, experts), (2, experts, pairs)
     cored = (2, experts, 2 * pairs)
     return pl.pallas_call(
         functools.partial(dispatch_kernel, experts, pairs),
-        out_shape=(shape, shape),
-        in_specs=vmem(1),
-        out_specs=tuple(vmem(2)),
+        out_shape=(
+            shape,
+            shape,
+            jax.ShapeDtypeStruct((experts * capacity, tokens), jnp.bfloat16),
+            jax.ShapeDtypeStruct(halo, jnp.float32),
+        ),
+        in_specs=vmem(5),
+        out_specs=tuple(vmem(4)),
         scratch_shapes=[
+            pltpu.VMEM((2, experts, capacity, width), jnp.bfloat16),
+            pltpu.VMEM(halo, jnp.float32),
+        ]
+        + [
             sems(*s)
-            for s in (flat, flat, flat, flat, rowed, rowed, rowed, rowed, cored, cored, (2,))
+            for s in (
+                flat, flat, flat, flat, rowed, rowed, rowed, rowed, cored, cored,
+                (2,), (1,), (1,),
+            )
         ],
         compiler_params=pltpu.CompilerParams(
             collective_id=0, has_side_effects=True, vmem_limit_bytes=32 * 1024 * 1024
         ),
-    )(sent)
-
-
-def give_back(part, select_t, cotangent, conv_out, experts, tp_count):
+    )(routes.T, route_weights.T, stream, cotangent, mixed)
+
+
+def give_back(part, select, cotangent, conv_out, conv_sum, outer, inner, given, taps,
+              out_weight, experts, tp_count):
     pairs = tp_count // 2
     _, _, capacity, model_width = part.shape
     tokens, channels = conv_out.shape
     width = model_width // tp_count
-    groups = 2 * experts
+    slice_width = model_width // (2 * experts)
+    border = min(8, tokens)
     most = max(pairs, 2 * (pairs - 1))
     late = max(pairs - 1, 1)
     bf16 = jnp.bfloat16
+    own_channels = jax.ShapeDtypeStruct((tokens, channels), bf16)
     return pl.pallas_call(
         functools.partial(return_kernel, experts, pairs),
         out_shape=(
-            jax.ShapeDtypeStruct((tokens, model_width), bf16),
-            jax.ShapeDtypeStruct((2, experts, tokens, model_width // groups), bf16),
-            jax.ShapeDtypeStruct((2, experts, tokens, channels), bf16),
+            jax.ShapeDtypeStruct((slice_width, channels), jnp.float32),
+            own_channels,
+            own_channels,
+            own_channels,
         ),
-        in_specs=vmem(4),
-        out_specs=tuple(vmem(3)),
+        in_specs=vmem(10),
+        out_specs=tuple(vmem(4)),
         scratch_shapes=[
+            pltpu.VMEM((tokens, model_width), bf16),
+            pltpu.VMEM((2, experts, tokens, slice_width), bf16),
+            pltpu.VMEM((2, experts, tokens, channels), bf16),
+            pltpu.VMEM((tokens + border, channels), jnp.float32),
+            pltpu.VMEM((border, channels), jnp.float32),
             pltpu.VMEM((2, pairs, experts, capacity, width), bf16),
             pltpu.VMEM((2, pairs, experts, capacity, width), bf16),
             pltpu.VMEM((experts, most, capacity, width), bf16),
@@ -392,7 +492,7 @@
             sems(*s)
             for shape in (
                 (2, pairs, experts), (experts, most), (experts, late), (experts,),
-                (2 * pairs,), (experts, 2), (experts,), (experts,),
+                (2 * pairs,), (experts, 2), (experts,), (experts,), (1,),
             )
             for s in (shape, shape)
         ]
@@ -400,7 +500,7 @@
         compiler_params=pltpu.CompilerParams(
             collective_id=1, has_side_effects=True, vmem_limit_bytes=40 * 1024 * 1024
         ),
-    )(part, select_t, cotangent, conv_out)
+    )(part, select, cotangent, conv_out, conv_sum, outer, inner, given, taps, out_weight)
 
 
 def per_device(
@@ -426,33 +526,40 @@
     slot_total = experts * capacity
     contract_first = (((0,), (0,)), ((), ()))
     contract_last = (((1,), (1,)), ((), ()))
-    flat_routes = routes.reshape(-1)
-    choose = (flat_routes[:, None] == jnp.arange(experts, dtype=jnp.int32)[None, :]).astype(
-        jnp.int32
-    )
-    before = jnp.cumsum(choose, axis=0) - choose
-    slot_place = flat_routes * capacity + jnp.sum(before * choose, axis=1)
-    slot_table = (jnp.arange(slot_total, dtype=jnp.int32)[:, None] == slot_place[None, :]).astype(
-        jnp.float32
-    )
-    select = jnp.sum(slot_table.reshape(slot_total, tok_rows, 2), axis=2).astype(jnp.bfloat16)
-    slot_weight = jnp.sum(slot_table * route_weights.reshape(-1)[None, :], axis=1)
     block_width = model_width // tp_count
-    offset = lax.axis_index("tp") * block_width
-    rows_part = lax.dynamic_slice_in_dim(stream, offset, block_width, 1)
-    cot_part = lax.dynamic_slice_in_dim(cotangent, offset, block_width, 1)
-    sent_rows = jnp.dot(select, rows_part, preferred_element_type=jnp.float32).astype(jnp.bfloat16)
-    sent_cot = (
-        jnp.dot(select, cot_part, preferred_element_type=jnp.float32) * slot_weight[:, None]
-    ).astype(jnp.bfloat16)
+    slots = groups * capacity
     direct = tp_count % 2 == 0 and capacity % 16 == 0 and block_width % 128 == 0
-    slots = groups * capacity
+    taps = conv_taps.astype(jnp.float32)
+    outer_f = outer_gate.astype(jnp.float32)
+    inner_f = inner_gate.astype(jnp.float32)
+    input_f = conv_input.astype(jnp.float32)
+    mixed = inner_f * input_f
     if direct:
-        sent = jnp.stack([sent_rows, sent_cot]).reshape(2, experts, capacity, block_width)
-        routed_rows, routed_cot = dispatch(sent, experts, tp_count)
+        routed_rows, routed_cot, select, early = dispatch(
+            routes, route_weights, stream, cotangent, mixed, capacity, experts, tp_count
+        )
         routed_rows = routed_rows.reshape(slots, model_width)
         routed_cot = routed_cot.reshape(slots, model_width)
+        earlier = jnp.where(lax.axis_index("sp") == 0, 0.0, early[-2:])
     else:
+        flat_routes = routes.reshape(-1)
+        choose = (flat_routes[:, None] == jnp.arange(experts, dtype=jnp.int32)[None, :]).astype(
+            jnp.int32
+        )
+        before = jnp.cumsum(choose, axis=0) - choose
+        slot_place = flat_routes * capacity + jnp.sum(before * choose, axis=1)
+        slot_table = (jnp.arange(slot_total, dtype=jnp.int32)[:, None] == slot_place[None, :]).astype(
+            jnp.float32
+        )
+        select = jnp.sum(slot_table.reshape(slot_total, tok_rows, 2), axis=2).astype(jnp.bfloat16)
+        slot_weight = jnp.sum(slot_table * route_weights.reshape(-1)[None, :], axis=1)
+        offset = lax.axis_index("tp") * block_width
+        rows_part = lax.dynamic_slice_in_dim(stream, offset, block_width, 1)
+        cot_part = lax.dynamic_slice_in_dim(cotangent, offset, block_width, 1)
+        sent_rows = jnp.dot(select, rows_part, preferred_element_type=jnp.float32).astype(jnp.bfloat16)
+        sent_cot = (
+            jnp.dot(select, cot_part, preferred_element_type=jnp.float32) * slot_weight[:, None]
+        ).astype(jnp.bfloat16)
         sent_rows = jnp.repeat(sent_rows.reshape(experts, capacity, -1), 2, axis=0)
         sent_cot = jnp.repeat(sent_cot.reshape(experts, capacity, -1), 2, axis=0)
         recv_rows, recv_cot = (
@@ -465,6 +572,7 @@
         )
         routed_rows = recv_rows.reshape(slots, model_width)
         routed_cot = recv_cot.reshape(slots, model_width)
+        earlier = from_behind(mixed[-2:], "sp", 1)
     gate_local = gate_weight[0]
     up_local = up_weight[0]
     down_local = down_weight[0]
@@ -495,29 +603,23 @@
     row_partial = row_partial + lax.dot_general(
         up_delta, up_local, contract_last, preferred_element_type=jnp.float32
     )
-    taps = conv_taps.astype(jnp.float32)
-    outer_f = outer_gate.astype(jnp.float32)
-    inner_f = inner_gate.astype(jnp.float32)
-    input_f = conv_input.astype(jnp.float32)
-    mixed = inner_f * input_f
-    earlier = from_behind(mixed[-2:], "sp", 1)
     padded = jnp.concatenate([earlier, mixed], axis=0)
     conv_sum = taps[0] * padded[:-2] + taps[1] * padded[1:-1] + taps[2] * padded[2:]
     conv_out = (outer_f * conv_sum).astype(jnp.bfloat16)
     if direct:
-        stream_grad, grad_all, conv_all = give_back(
+        out_grad, outer_grad, inner_grad, input_grad = give_back(
             row_partial.astype(jnp.bfloat16).reshape(2, experts, capacity, model_width),
-            select.T,
+            select,
             cotangent,
             conv_out,
+            conv_sum,
+            outer_gate,
+            inner_gate,
+            conv_input,
+            taps,
+            out_weight,
             experts,
             tp_count,
-        )
-        out_grad = lax.dot_general(
-            grad_all.reshape(groups * tok_rows, -1),
-            conv_all.reshape(groups * tok_rows, -1),
-            contract_first,
-            preferred_element_type=jnp.float32,
         )
     else:
         half_sums = lax.psum_scatter(
@@ -543,14 +645,14 @@
             scatter_dimension=0,
             tiled=True,
         ).astype(jnp.float32)
-    conv_grad = jnp.dot(stream_grad, out_weight, preferred_element_type=jnp.float32)
-    outer_grad = (conv_grad * conv_sum).astype(jnp.bfloat16)
-    scaled = conv_grad * outer_f
-    later = from_behind(scaled[:2], "sp", -1)
-    extended = jnp.concatenate([scaled, later], axis=0)
-    mixed_grad = taps[2] * extended[:-2] + taps[1] * extended[1:-1] + taps[0] * extended[2:]
-    inner_grad = (mixed_grad * input_f).astype(jnp.bfloat16)
-    input_grad = (mixed_grad * inner_f).astype(jnp.bfloat16)
+        conv_grad = jnp.dot(stream_grad, out_weight, preferred_element_type=jnp.float32)
+        outer_grad = (conv_grad * conv_sum).astype(jnp.bfloat16)
+        scaled = conv_grad * outer_f
+        later = from_behind(scaled[:2], "sp", -1)
+        extended = jnp.concatenate([scaled, later], axis=0)
+        mixed_grad = taps[2] * extended[:-2] + taps[1] * extended[1:-1] + taps[0] * extended[2:]
+        inner_grad = (mixed_grad * input_f).astype(jnp.bfloat16)
+        input_grad = (mixed_grad * inner_f).astype(jnp.bfloat16)
     return (gate_grad, up_grad, down_grad, out_grad, outer_grad, inner_grad, input_grad)
 
 

time: 126 us -> 119 us (0.944)
  local copies, waits for them, and re-layouts: 2.65 us -> 9.19 us
  starting transfers between devices: 6.15 us -> 0 us
  other arithmetic: 4.78 us -> 1.1 us
  waiting for transfers between devices: 3.14 us -> 0 us
  matrix products: 23.6 us -> 21 us
  Pallas kernels: 84.6 us -> 86.8 us
    unnamed x20 -> x32, local copies, waits for them, and re-layouts: 1.63 us -> 9.19 us
    ppermute x2 -> x0, starting transfers between devices: 6.15 us -> none  [from_behind(): return lax.ppermute(block, axis, route)]
    dot_general x4 -> x0, matrix products: 4.37 us -> none  [the longest x1 1.19 us: per_device(): jnp.dot(select, cot_part, preferred_element_type=jnp.float32)]
    ppermute x2 -> x0, waiting for transfers between devices: 3.14 us -> none  [from_behind(): return lax.ppermute(block, axis, route)]
    pallas_call x1, Pallas kernels: 39.5 us -> 42.2 us  [dispatch(): pl.pallas_call(functools.partial(dispatch_kernel, experts, pairs), out_sh...]
    dot_general x1, matrix products: 2.03 us -> 3.66 us  [per_device(): lax.dot_general(up_delta, up_local, contract_last, preferred_element_type...]
    another operation x3 -> x0, other arithmetic: 1.34 us -> none
    convert_element_type x3 -> x1, other arithmetic: 1.33 us -> 0.01 us  [per_device(): taps = conv_taps.astype(jnp.float32)]
  transfers between devices with their start and end apart: 2 -> 0, of which waited for: 1 -> 0; matrix products, arithmetic and copies ran while one was open for 22% -> 0% of each run, Pallas kernels for 31% -> 0%
where the time goes in v2:
time: 119 us
  Pallas kernels  86.8 us (73%)
  matrix products  21 us (18%)
  local copies, waits for them, and re-layouts  9.19 us (8%)
    pallas_call x1, Pallas kernels, give_back(): pl.pallas_call(functools.partial(return_kernel, experts, pairs), out_shap...  44.6 us
    pallas_call x1, Pallas kernels, dispatch(): pl.pallas_call(functools.partial(dispatch_kernel, experts, pairs), out_sh...  42.2 us
    unnamed x32, local copies, waits for them, and re-layouts  9.19 us
    dot_general x1, matrix products, per_device(): lax.dot_general(up_delta, up_local, contract_last, preferred_element_type...  3.66 us
    dot_general x1, matrix products, per_device(): lax.dot_general(hidden, routed_cot, contract_first, preferred_element_typ...  3.3 us
    dot_general x1, matrix products, per_device(): lax.dot_general(routed_rows, up_delta, contract_first, preferred_element_...  3.19 us
    dot_general x1, matrix products, per_device(): lax.dot_general(routed_rows, gate_delta, contract_first, preferred_elemen...  3.19 us

profile of v2, /device:TPU:0, one launch (start us, length us, event | category | flops | bytes accessed | tf_op | source)
XLA Modules:
  0.0 118.9 jit_solution(9444967929846786835)
XLA Ops:
  0.6 0.0 copy-start
  0.6 1.0 convert_multiply_fusion.mixed_ref
  1.7 0.0 copy-start.2
  1.7 1.0 copy-done.2
  2.7 0.0 copy-start.5
  2.7 1.0 copy-done.5
  3.8 0.0 copy-start.9
  3.8 0.7 copy-done.9
  4.5 0.0 copy-start.10
  4.5 0.7 copy-done.10
  5.1 42.2 %shard_map.171 = (bf16[2,4,96,2048]{3,2,1,0:T(8,128)(2,1)S(1)}, bf16[2,4,96,2048]{3,2,1,0:T(8,128)(2,1)S(1)}, bf16[384,128]{1,0:T(8,128)(2,1)S(1)}, f32[8,256]{1,0:T(8,128)S(1)}) custom-call(s32[2,128]{1,0:T(2,128)S(1)} %bitcast.40, f32[2,128]{1,0:T(2,128)S(1)} %bitcast.41, bf16[128,2048]{1,0:T(8,128)(2,1)S(1)} %copy-done.5, ...), custom_call_target="tpu_custom_call" | custom-call | tf_op jit(solution)/shard_map/pallas_call | solution.py:428
  47.3 0.0 copy-done
  47.3 0.0 copy-start.11
  47.3 1.8 %fusion.5 = f32[768,512]{1,0:T(8,128)S(1)} fusion(bf16[768,2048]{1,0:T(8,128)(2,1)S(1)} %bitcast.44, bf16[1,2048,512]{2,1,0:T(8,128)(2,1)S(1)} %copy-done), kind=kOutput, calls=%fused_computation.9 | convolution fusion | flops 1610612736 | bytes 6815744 | tf_op jit(solution)/shard_map/dot_general | solution.py:579
  49.1 0.0 copy-done.11
  49.1 0.0 copy-start.13
  49.1 1.8 %fusion.8 = f32[768,512]{1,0:T(8,128)S(1)} fusion(bf16[768,2048]{1,0:T(8,128)(2,1)S(1)} %bitcast.45, bf16[1,2048,512]{2,1,0:T(8,128)(2,1)S(1)} %copy-done.11), kind=kOutput, calls=%fused_computation.12 | convolution fusion | flops 1610612736 | bytes 6815744 | tf_op jit(solution)/shard_map/dot_general | solution.py:580
  50.9 0.0 copy-done.13
  50.9 2.3 %multiply_convert_fusion.1 = (bf16[768,512]{1,0:T(8,128)(2,1)S(1)}, bf16[768,512]{1,0:T(8,128)(2,1)S(1)}) fusion(f32[768,512]{1,0:T(8,128)S(1)} %fusion.5, f32[768,512]{1,0:T(8,128)S(1)} %fusion.8, bf16[768,2048]{1,0:T(8,128)(2,1)S(1)} %bitcast.42, bf16[1,512,2048]{2,1,0:T(8,128)(2,1)S(1)} %copy-done.13), kind=kOutput, calls=%fused_computation.17 | convolution fusion | flops 1615724544 | bytes 9961472 | tf_op jit(solution)/shard_map/dot_general | solution.py:581
  53.2 3.2 %fusion = bf16[1,2048,512]{2,1,0:T(8,128)(2,1)} fusion(bf16[768,2048]{1,0:T(8,128)(2,1)S(1)} %bitcast.46, bf16[768,512]{1,0:T(8,128)(2,1)S(1)} %get-tuple-element.26), kind=kOutput, calls=%fused_computation.4 | convolution fusion | flops 1611661312 | bytes 6029312 | tf_op jit(solution)/shard_map/dot_general | solution.py:591
  56.4 3.2 %fusion.1 = bf16[1,2048,512]{2,1,0:T(8,128)(2,1)} fusion(bf16[768,2048]{1,0:T(8,128)(2,1)S(1)} %bitcast.47, bf16[768,512]{1,0:T(8,128)(2,1)S(1)} %get-tuple-element.25), kind=kOutput, calls=%fused_computation.5 | convolution fusion | flops 1611661312 | bytes 6029312 | tf_op jit(solution)/shard_map/dot_general | solution.py:594
  59.6 3.3 %fusion.2 = bf16[1,512,2048]{2,1,0:T(8,128)(2,1)} fusion(bf16[768,2048]{1,0:T(8,128)(2,1)S(1)} %bitcast.43, f32[768,512]{1,0:T(8,128)S(1)} %fusion.8, f32[768,512]{1,0:T(8,128)S(1)} %fusion.5), kind=kOutput, calls=%fused_computation.6 | convolution fusion | flops 1614020608 | bytes 8388608 | tf_op jit(solution)/shard_map/dot_general | solution.py:597
  62.9 1.8 %fusion.3 = f32[768,2048]{1,0:T(8,128)S(1)} fusion(bf16[768,512]{1,0:T(8,128)(2,1)S(1)} %get-tuple-element.26, bf16[1,2048,512]{2,1,0:T(8,128)(2,1)S(1)} %copy-done), kind=kOutput, calls=%fused_computation.7 | convolution fusion | flops 1610612736 | bytes 9175040 | tf_op jit(solution)/shard_map/dot_general | solution.py:600
  64.7 0.0 copy-start.12
  64.7 0.0 copy-start.6
  64.7 0.0 copy-start.3
  64.8 0.0 copy-start.7
  64.8 0.0 copy-start.8
  64.8 3.7 %add_convert_fusion = bf16[768,2048]{1,0:T(8,128)(2,1)} fusion(f32[768,2048]{1,0:T(8,128)S(1)} %fusion.3, bf16[768,512]{1,0:T(8,128)(2,1)S(1)} %get-tuple-element.25, bf16[1,2048,512]{2,1,0:T(8,128)(2,1)S(1)} %copy-done.11), kind=kOutput, calls=%fused_computation | convolution fusion | flops 1613758464 | bytes 12320768 | tf_op jit(solution)/shard_map/dot_general | solution.py:603
  68.4 0.0 copy-done.12
  68.5 0.0 copy-done.6
  68.5 0.1 multiply_convert_fusion.4
  68.5 0.0 copy-done.3
  68.5 0.0 copy-done.7
  68.6 0.0 copy-done.8
  68.6 0.0 copy-start.1
  68.6 1.9 %copy-done.1 = bf16[768,2048]{1,0:T(8,128)(2,1)S(1)} copy-done((bf16[768,2048]{1,0:T(8,128)(2,1)S(1)}, bf16[768,2048]{1,0:T(8,128)(2,1)}, u32[]{:S(2)}) %copy-start.1) | copy-done | bytes 3145752
  70.5 0.0 copy-start.4
  70.5 1.2 %copy-done.4 = bf16[2048,256]{1,0:T(8,128)(2,1)S(1)} copy-done((bf16[2048,256]{1,0:T(8,128)(2,1)S(1)}, bf16[2048,256]{1,0:T(8,128)(2,1)}, u32[]{:S(2)}) %copy-start.4) | copy-done | bytes 1048600
  71.7 44.6 %shard_map.172 = (f32[256,256]{1,0:T(8,128)S(1)}, bf16[128,256]{1,0:T(8,128)(2,1)S(1)}, bf16[128,256]{1,0:T(8,128)(2,1)S(1)}, bf16[128,256]{1,0:T(8,128)(2,1)S(1)}) custom-call(bf16[2,4,96,2048]{3,2,1,0:T(8,128)(2,1)S(1)} %bitcast.39, bf16[384,128]{1,0:T(8,128)(2,1)S(1)} %get-tuple-element.17.sel_ref, bf16[128,2048]{1,0:T(8,128)(2,1)S(1)} %copy-done.3, ...), custom_call_target="tpu_custom_call" | custom-call | tf_op jit(solution)/shard_map/pallas_call | solution.py:467
  116.3 0.7 copy.23
  117.0 0.6 copy.24
  117.6 0.6 copy.25
  118.3 0.6 copy.26
  (3 shorter events, 0.0 us)
Async XLA Ops:
  0.6 46.7 %copy-start = (bf16[1,2048,512]{2,1,0:T(8,128)(2,1)S(1)}, bf16[1,2048,512]{2,1,0:T(8,128)(2,1)}, u32[]{:S(2)}) copy-start(bf16[1,2048,512]{2,1,0:T(8,128)(2,1)} %param.16) | copy-start | bytes 6291460
  1.7 1.0 copy-start.2
  2.7 1.0 copy-start.5
  3.8 0.7 copy-start.9
  4.5 0.7 copy-start.10
  47.3 1.8 %copy-start.11 = (bf16[1,2048,512]{2,1,0:T(8,128)(2,1)S(1)}, bf16[1,2048,512]{2,1,0:T(8,128)(2,1)}, u32[]{:S(2)}) copy-start(bf16[1,2048,512]{2,1,0:T(8,128)(2,1)} %param.17) | copy-start | bytes 6291460
  49.1 1.8 %copy-start.13 = (bf16[1,512,2048]{2,1,0:T(8,128)(2,1)S(1)}, bf16[1,512,2048]{2,1,0:T(8,128)(2,1)}, u32[]{:S(2)}) copy-start(bf16[1,512,2048]{2,1,0:T(8,128)(2,1)} %param.18) | copy-start | bytes 6291460
  64.7 3.7 %copy-start.12 = (bf16[3,256]{1,0:T(4,128)(2,1)S(1)}, bf16[3,256]{1,0:T(4,128)(2,1)}, u32[]{:S(2)}) copy-start(bf16[3,256]{1,0:T(4,128)(2,1)} %param.22) | copy-start | bytes 4612
  64.7 3.7 %copy-start.6 = (bf16[128,256]{1,0:T(8,128)(2,1)S(1)}, bf16[128,256]{1,0:T(8,128)(2,1)}, u32[]{:S(2)}) copy-start(bf16[128,256]{1,0:T(8,128)(2,1)} %outer_ref.1) | copy-start | bytes 196612
  64.7 3.8 %copy-start.3 = (bf16[128,2048]{1,0:T(8,128)(2,1)S(1)}, bf16[128,2048]{1,0:T(8,128)(2,1)}, u32[]{:S(2)}) copy-start(bf16[128,2048]{1,0:T(8,128)(2,1)} %cot_ref.1) | copy-start | bytes 1572868
  64.8 3.8 %copy-start.7 = (bf16[128,256]{1,0:T(8,128)(2,1)S(1)}, bf16[128,256]{1,0:T(8,128)(2,1)}, u32[]{:S(2)}) copy-start(bf16[128,256]{1,0:T(8,128)(2,1)} %input_ref.1) | copy-start | bytes 196612
  64.8 3.8 %copy-start.8 = (bf16[128,256]{1,0:T(8,128)(2,1)S(1)}, bf16[128,256]{1,0:T(8,128)(2,1)}, u32[]{:S(2)}) copy-start(bf16[128,256]{1,0:T(8,128)(2,1)} %inner_ref.1) | copy-start | bytes 196612
  68.6 1.9 %copy-start.1 = (bf16[768,2048]{1,0:T(8,128)(2,1)S(1)}, bf16[768,2048]{1,0:T(8,128)(2,1)}, u32[]{:S(2)}) copy-start(bf16[768,2048]{1,0:T(8,128)(2,1)} %add_convert_fusion) | copy-start | bytes 9437188
  70.5 1.2 %copy-start.4 = (bf16[2048,256]{1,0:T(8,128)(2,1)S(1)}, bf16[2048,256]{1,0:T(8,128)(2,1)}, u32[]{:S(2)}) copy-start(bf16[2048,256]{1,0:T(8,128)(2,1)} %weight_ref.1) | copy-start | bytes 3145732

commit v3 on v2

--- a/solution.py
+++ b/solution.py
@@ -76,9 +76,10 @@
     return lambda: pl.semaphore_wait(barrier, len(peers))
 
 
-def dispatch_kernel(experts, pairs, routes_ref, weights_ref, stream_ref, given_ref, mixed_ref,
+def dispatch_kernel(experts, pairs, routes_hbm, weights_hbm, stream_hbm, given_hbm, inner_hbm, input_hbm,
                     rows_ref, cot_ref, select_ref, early_ref, send_ref, tail_ref,
-                    zs, zr, xs, xr, ys, yr, ds, dr, cs, cr, own, hs, hr):
+                    routes_ref, weights_ref, block_ref, edge_ref,
+                    zs, zr, xs, xr, ys, yr, ds, dr, cs, cr, own, hs, hr, ls):
     seat = Seat(experts, pairs)
     capacity, width = send_ref.shape[2:]
     tokens = routes_ref.shape[1]
@@ -91,7 +92,24 @@
         + [seat.other_row(seat.row_ahead(d)) for d in range(1, pairs)]
     )
     started = []
-    tail_ref[...] = mixed_ref[tokens - tail_ref.shape[0]:, :]
+    mine = pl.ds(pl.multiple_of(seat.tp * width, width), width)
+    edge = pl.ds(tokens - tail_ref.shape[0], tail_ref.shape[0])
+    loads = [
+        pltpu.make_async_copy(src, dst, ls.at[n])
+        for n, (src, dst) in enumerate((
+            (routes_hbm, routes_ref),
+            (weights_hbm, weights_ref),
+            (stream_hbm.at[:, mine], block_ref.at[0]),
+            (inner_hbm.at[edge, :], edge_ref.at[0]),
+            (input_hbm.at[edge, :], edge_ref.at[1]),
+            (given_hbm.at[:, mine], block_ref.at[1]),
+        ))
+    ]
+    for load in loads:
+        load.start()
+    for load in loads:
+        load.wait()
+    tail_ref[...] = edge_ref[0].astype(jnp.float32) * edge_ref[1].astype(jnp.float32)
     number = lax.broadcasted_iota(jnp.int32, (experts, tokens), 0)
     named = [routes_ref[k:k + 1, :] == number for k in range(2)]
     member = jnp.where(named[0] | named[1], 1.0, 0.0)
@@ -107,7 +125,6 @@
         preferred_element_type=jnp.float32,
     )
     slot = lax.broadcasted_iota(jnp.int32, (capacity, tokens), 0).astype(jnp.float32)
-    mine = pl.ds(pl.multiple_of(seat.tp * width, width), width)
     slot_weight = []
     for e in range(experts):
         chosen = jnp.where(slot == rank[e:e + 1], member[e:e + 1], 0.0)
@@ -115,7 +132,7 @@
         select_ref[e * capacity:(e + 1) * capacity, :] = chosen.astype(jnp.bfloat16)
 
     def fill(kind):
-        block = stream_ref[:, mine] if kind == 0 else given_ref[:, mine]
+        block = block_ref[kind]
         for e in range(experts):
             picked = jnp.dot(
                 select_ref[e * capacity:(e + 1) * capacity, :], block,
@@ -213,10 +230,11 @@
         copy.wait()
 
 
-def return_kernel(experts, pairs, part_ref, sel_ref, cot_ref, conv_ref, sum_ref, outer_ref,
-                  inner_ref, input_ref, taps_ref, weight_ref,
-                  out_grad_ref, outer_grad_ref, inner_grad_ref, input_grad_ref,
-                  sg_ref, g_ref, c_ref, ext_ref, late_ref, a_ref, acc_ref, b1_ref, acc2_ref, b2_ref, fin_ref, ret_ref,
+def return_kernel(experts, pairs, part_ref, sel_ref, cot_hbm, conv_ref, sum_ref, outer_ref,
+                  inner_ref, input_ref, taps_ref, weight_hbm,
+                  rows_ref, routed_ref, hidden_ref, gate_ref, up_ref,
+                  gate_grad_ref, up_grad_ref, down_grad_ref, out_grad_ref, outer_grad_ref, inner_grad_ref, input_grad_ref,
+                  cot_ref, weight_ref, sg_ref, g_ref, c_ref, ext_ref, late_ref, a_ref, acc_ref, b1_ref, acc2_ref, b2_ref, fin_ref, ret_ref,
                   as_, ar, b1s, b1r, b2s, b2r, zs, zr, ms, mr, gs, gr, vs, vr, us, ur, hs, hr, own):
     seat = Seat(experts, pairs)
     capacity = part_ref.shape[2]
@@ -235,6 +253,24 @@
         + [seat.other_row(seat.row_ahead(d)) for d in range(1, pairs)]
     )()
     started = []
+    over_first = (((0,), (0,)), ((), ()))
+    step = 512 if rows_ref.shape[1] % 512 == 0 else rows_ref.shape[1]
+    pieces = [(n, at) for n in range(3) for at in range(0, rows_ref.shape[1], step)]
+
+    def work(count):
+        for n, at in [pieces.pop(0) for _ in range(min(count, len(pieces)))]:
+            span = slice(at, at + step)
+            if n < 2:
+                delta, out = ((gate_ref, gate_grad_ref), (up_ref, up_grad_ref))[n]
+                out[span, :] = lax.dot_general(
+                    rows_ref[:, span], delta[...], over_first,
+                    preferred_element_type=jnp.float32,
+                ).astype(jnp.bfloat16)
+            else:
+                down_grad_ref[:, span] = lax.dot_general(
+                    hidden_ref[...], routed_ref[:, span], over_first,
+                    preferred_element_type=jnp.float32,
+                ).astype(jnp.bfloat16)
 
     def cols(tp):
         return pl.ds(pl.multiple_of(tp * width, width), width)
@@ -264,6 +300,11 @@
                      seat.other_core())
     copy_conv = pltpu.make_async_copy(conv_ref, c_ref.at[seat.half, seat.expert], own.at[0])
     copy_conv.start()
+    mine = cols(seat.tp)
+    load_cot = pltpu.make_async_copy(cot_hbm.at[:, mine], cot_ref, own.at[2])
+    load_weight = pltpu.make_async_copy(weight_hbm, weight_ref, own.at[3])
+    load_cot.start()
+    load_weight.start()
     for k in range(1, experts):
         push(conv_ref, c_ref.at[seat.half, seat.expert], vs.at[k], vr.at[k],
              seat.other_expert(seat.behind(offs[k])))
@@ -324,6 +365,7 @@
     for n in range(experts + 2):
         if n < experts:
             first(order[n])
+        work(1)
         if 1 <= n <= experts:
             second(order[n - 1])
         if n >= 2:
@@ -335,19 +377,21 @@
         if k:
             landed(spot, vs.at[k], vr.at[k])
         push(spot, spot, us.at[k], ur.at[k], seat.other_half())
+    work(2)
+    load_cot.wait()
+    load_weight.wait()
     for k in range(1, experts):
         rows = pl.ds(pl.multiple_of(seat.ahead(offs[k]) * capacity, 16), capacity)
         landed(ret_ref.at[rows, :], zs.at[k], zr.at[k])
-    over_first = (((0,), (0,)), ((), ()))
     moe = lax.dot_general(
         sel_ref[...], ret_ref[...], over_first, preferred_element_type=jnp.float32
     )
-    mine = cols(seat.tp)
-    sg_ref[:, mine] = total(cot_ref[:, mine], moe.astype(jnp.bfloat16))
+    sg_ref[:, mine] = total(cot_ref[...], moe.astype(jnp.bfloat16))
     for d in range(1, pairs):
         push(sg_ref.at[:, mine], sg_ref.at[:, mine], ms.at[2 * d], mr.at[2 * d],
              seat.other_row(seat.row_behind(d)))
     push(sg_ref.at[:, mine], sg_ref.at[:, mine], ms.at[0], mr.at[0], seat.other_core())
+    work(2)
     for d in range(1, pairs):
         theirs = sg_ref.at[:, cols(seat.row_ahead(d) * 2 + seat.core)]
         landed(theirs, ms.at[2 * d], mr.at[2 * d])
@@ -386,6 +430,7 @@
         )
 
     add_out(seat.half, seat.expert)
+    work(len(pieces))
     landed(late_ref, hs.at[0], hr.at[0])
     ext_ref[tokens:tokens + border, :] = jnp.where(
         seat.sp == 2 * experts - 1, 0.0, late_ref[...]
@@ -412,17 +457,21 @@
     return [pl.BlockSpec(memory_space=pltpu.VMEM)] * count
 
 
+def hbm(count):
+    return [pl.BlockSpec(memory_space=pltpu.HBM)] * count
+
+
 def sems(*shape):
     return pltpu.SemaphoreType.DMA(shape)
 
 
-def dispatch(routes, route_weights, stream, cotangent, mixed, capacity, experts, tp_count):
+def dispatch(routes, route_weights, stream, cotangent, inner, given, capacity, experts, tp_count):
     pairs = tp_count // 2
     tokens, model_width = stream.shape
     width = model_width // tp_count
-    border = min(8, tokens)
+    border = min(16, tokens)
     shape = jax.ShapeDtypeStruct((2, experts, capacity, model_width), jnp.bfloat16)
-    halo = (border, mixed.shape[1])
+    halo = (border, inner.shape[1])
     flat, rowed = (2, experts), (2, experts, pairs)
     cored = (2, experts, 2 * pairs)
     return pl.pallas_call(
@@ -433,27 +482,31 @@
             jax.ShapeDtypeStruct((experts * capacity, tokens), jnp.bfloat16),
             jax.ShapeDtypeStruct(halo, jnp.float32),
         ),
-        in_specs=vmem(5),
+        in_specs=hbm(6),
         out_specs=tuple(vmem(4)),
         scratch_shapes=[
             pltpu.VMEM((2, experts, capacity, width), jnp.bfloat16),
             pltpu.VMEM(halo, jnp.float32),
+            pltpu.VMEM((2, tokens), jnp.int32),
+            pltpu.VMEM((2, tokens), jnp.float32),
+            pltpu.VMEM((2, tokens, width), jnp.bfloat16),
+            pltpu.VMEM((2,) + halo, jnp.bfloat16),
         ]
         + [
             sems(*s)
             for s in (
                 flat, flat, flat, flat, rowed, rowed, rowed, rowed, cored, cored,
-                (2,), (1,), (1,),
+                (2,), (1,), (1,), (6,),
             )
         ],
         compiler_params=pltpu.CompilerParams(
-            collective_id=0, has_side_effects=True, vmem_limit_bytes=32 * 1024 * 1024
+            collective_id=0, has_side_effects=True, vmem_limit_bytes=12 * 1024 * 1024
         ),
-    )(routes.T, route_weights.T, stream, cotangent, mixed)
+    )(routes.T, route_weights.T, stream, cotangent, inner, given)
 
 
 def give_back(part, select, cotangent, conv_out, conv_sum, outer, inner, given, taps,
-              out_weight, experts, tp_count):
+              out_weight, rows, routed, hidden, gate_delta, up_delta, experts, tp_count):
     pairs = tp_count // 2
     _, _, capacity, model_width = part.shape
     tokens, channels = conv_out.shape
@@ -463,18 +516,25 @@
     most = max(pairs, 2 * (pairs - 1))
     late = max(pairs - 1, 1)
     bf16 = jnp.bfloat16
+    units = hidden.shape[1]
+    gate_shape = jax.ShapeDtypeStruct((model_width, units), bf16)
     own_channels = jax.ShapeDtypeStruct((tokens, channels), bf16)
     return pl.pallas_call(
         functools.partial(return_kernel, experts, pairs),
         out_shape=(
+            gate_shape,
+            gate_shape,
+            jax.ShapeDtypeStruct((units, model_width), bf16),
             jax.ShapeDtypeStruct((slice_width, channels), jnp.float32),
             own_channels,
             own_channels,
             own_channels,
         ),
-        in_specs=vmem(10),
-        out_specs=tuple(vmem(4)),
+        in_specs=vmem(2) + hbm(1) + vmem(6) + hbm(1) + vmem(5),
+        out_specs=tuple(vmem(7)),
         scratch_shapes=[
+            pltpu.VMEM((tokens, width), bf16),
+            pltpu.VMEM((model_width, channels), bf16),
             pltpu.VMEM((tokens, model_width), bf16),
             pltpu.VMEM((2, experts, tokens, slice_width), bf16),
             pltpu.VMEM((2, experts, tokens, channels), bf16),
@@ -496,11 +556,14 @@
             )
             for s in (shape, shape)
         ]
-        + [sems(2)],
+        + [sems(4)],
         compiler_params=pltpu.CompilerParams(
-            collective_id=1, has_side_effects=True, vmem_limit_bytes=40 * 1024 * 1024
+            collective_id=1, has_side_effects=True, vmem_limit_bytes=18 * 1024 * 1024
         ),
-    )(part, select, cotangent, conv_out, conv_sum, outer, inner, given, taps, out_weight)
+    )(
+        part, select, cotangent, conv_out, conv_sum, outer, inner, given, taps, out_weight,
+        rows, routed, hidden, gate_delta, up_delta,
+    )
 
 
 def per_device(
@@ -536,7 +599,8 @@
     mixed = inner_f * input_f
     if direct:
         routed_rows, routed_cot, select, early = dispatch(
-            routes, route_weights, stream, cotangent, mixed, capacity, experts, tp_count
+            routes, route_weights, stream, cotangent, inner_gate, conv_input,
+            capacity, experts, tp_count,
         )
         routed_rows = routed_rows.reshape(slots, model_width)
         routed_cot = routed_cot.reshape(slots, model_width)
@@ -588,15 +652,6 @@
     gate_delta = (hidden_grad * up_pre * sigma * (1.0 + gate_pre * (1.0 - sigma))).astype(
         jnp.bfloat16
     )
-    gate_grad = lax.dot_general(
-        routed_rows, gate_delta, contract_first, preferred_element_type=jnp.float32
-    ).astype(jnp.bfloat16)[None]
-    up_grad = lax.dot_general(
-        routed_rows, up_delta, contract_first, preferred_element_type=jnp.float32
-    ).astype(jnp.bfloat16)[None]
-    down_grad = lax.dot_general(
-        hidden, routed_cot, contract_first, preferred_element_type=jnp.float32
-    ).astype(jnp.bfloat16)[None]
     row_partial = lax.dot_general(
         gate_delta, gate_local, contract_last, preferred_element_type=jnp.float32
     )
@@ -607,7 +662,7 @@
     conv_sum = taps[0] * padded[:-2] + taps[1] * padded[1:-1] + taps[2] * padded[2:]
     conv_out = (outer_f * conv_sum).astype(jnp.bfloat16)
     if direct:
-        out_grad, outer_grad, inner_grad, input_grad = give_back(
+        gate_grad, up_grad, down_grad, out_grad, outer_grad, inner_grad, input_grad = give_back(
             row_partial.astype(jnp.bfloat16).reshape(2, experts, capacity, model_width),
             select,
             cotangent,
@@ -618,10 +673,25 @@
             conv_input,
             taps,
             out_weight,
+            routed_rows,
+            routed_cot,
+            hidden,
+            gate_delta,
+            up_delta,
             experts,
             tp_count,
         )
+        gate_grad, up_grad, down_grad = gate_grad[None], up_grad[None], down_grad[None]
     else:
+        gate_grad = lax.dot_general(
+            routed_rows, gate_delta, contract_first, preferred_element_type=jnp.float32
+        ).astype(jnp.bfloat16)[None]
+        up_grad = lax.dot_general(
+            routed_rows, up_delta, contract_first, preferred_element_type=jnp.float32
+        ).astype(jnp.bfloat16)[None]
+        down_grad = lax.dot_general(
+            hidden, routed_cot, contract_first, preferred_element_type=jnp.float32
+        ).astype(jnp.bfloat16)[None]
         half_sums = lax.psum_scatter(
             row_partial.astype(jnp.bfloat16), "tp", scatter_dimension=1, tiled=True
         ).astype(jnp.float32)

time: 119 us -> 115 us (0.966)
  matrix products: 21 us -> 11.5 us
  local copies, waits for them, and re-layouts: 9.19 us -> 12.6 us
  other arithmetic: 1.1 us -> 2.48 us
    dot_general x3 -> x0, matrix products: 9.68 us -> none  [the longest x1 3.3 us: per_device(): lax.dot_general(hidden, routed_cot, contract_first, preferred_element_typ...]
    unnamed x32 -> x33, local copies, waits for them, and re-layouts: 9.19 us -> 11.7 us
    dot_general x1, matrix products: 3.66 us -> 1.86 us  [per_device(): lax.dot_general(up_delta, up_local, contract_last, preferred_element_type...]
    dot_general x1, matrix products: 2.28 us -> 3.56 us  [per_device(): lax.dot_general(routed_cot, down_local, contract_last, preferred_element_...]
where the time goes in v3:
time: 115 us; the launch traced here: 114 us
  Pallas kernels  86.9 us (76%)
  local copies, waits for them, and re-layouts  12.6 us (11%)
  matrix products  11.5 us (10%)
  other arithmetic  2.48 us (2%)
    pallas_call x1, Pallas kernels, give_back(): pl.pallas_call(functools.partial(return_kernel, experts, pairs), out_shap...  44.7 us
    pallas_call x1, Pallas kernels, dispatch(): pl.pallas_call(functools.partial(dispatch_kernel, experts, pairs), out_sh...  42.2 us
    unnamed x33, local copies, waits for them, and re-layouts  11.7 us
    dot_general x1, matrix products, per_device(): lax.dot_general(routed_cot, down_local, contract_last, preferred_element_...  3.56 us
    dot_general x1, matrix products, per_device(): up_pre = jnp.dot(routed_rows, up_local, preferred_element_type=jnp.float32)  2.45 us

profile of v3, /device:TPU:0, one launch (start us, length us, event | category | flops | bytes accessed | tf_op | source)
XLA Modules:
  0.0 114.3 jit_solution(10959293795886815342)
XLA Ops:
  0.6 0.0 copy-start
  0.7 0.9 fusion.16
  1.5 0.7 convert_element_type.31.taps_ref
  2.2 0.9 convert_multiply_fusion
  3.1 0.0 copy-start.1
  3.1 1.0 copy-done.1
  4.1 0.0 copy-start.4
  4.1 0.8 copy-done.4
  5.0 0.0 copy-start.6
  5.0 0.8 copy-done.6
  5.8 0.0 copy-start.8
  5.8 1.0 copy-done.8
  6.9 0.0 copy-start.10
  6.9 0.7 copy-done.10
  7.5 0.0 copy-start.11
  7.5 0.7 copy-done.11
  8.2 42.2 %shard_map.171 = (bf16[2,4,96,2048]{3,2,1,0:T(8,128)(2,1)S(1)}, bf16[2,4,96,2048]{3,2,1,0:T(8,128)(2,1)S(1)}, bf16[384,128]{1,0:T(8,128)(2,1)S(1)}, f32[16,256]{1,0:T(8,128)S(1)}) custom-call(s32[2,128]{1,0:T(2,128)S(1)} %bitcast.40, f32[2,128]{1,0:T(2,128)S(1)} %bitcast.41, bf16[128,2048]{1,0:T(8,128)(2,1)S(1)} %copy-done.8, ...), custom_call_target="tpu_custom_call" | custom-call | tf_op jit(solution)/shard_map/pallas_call | solution.py:477
  50.5 0.9 multiply_convert_fusion.3
  51.4 0.0 copy-start.12
  51.4 3.6 %fusion.7 = f32[768,512]{1,0:T(8,128)S(1)} fusion(bf16[768,2048]{1,0:T(8,128)(2,1)S(1)} %bitcast.35, bf16[1,512,2048]{2,1,0:T(8,128)(2,1)} %param.18), kind=kOutput, calls=%fused_computation.8 | convolution fusion | flops 1610612736 | bytes 6815744 | tf_op jit(solution)/shard_map/dot_general | solution.py:645
  54.9 0.0 copy-done.12
  54.9 1.8 %fusion.2 = f32[768,512]{1,0:T(8,128)S(1)} fusion(bf16[768,2048]{1,0:T(8,128)(2,1)S(1)} %bitcast.32, bf16[1,2048,512]{2,1,0:T(8,128)(2,1)S(1)} %copy-done.12), kind=kOutput, calls=%fused_computation.3 | convolution fusion | flops 1610612736 | bytes 6815744 | tf_op jit(solution)/shard_map/dot_general | solution.py:643
  56.7 0.0 copy-done
  56.7 2.5 %multiply_convert_fusion = (bf16[768,512]{1,0:T(8,128)(2,1)S(1)}, bf16[768,512]{1,0:T(8,128)(2,1)S(1)}, bf16[768,512]{1,0:T(8,128)(2,1)S(1)}) fusion(f32[768,512]{1,0:T(8,128)S(1)} %fusion.2, f32[768,512]{1,0:T(8,128)S(1)} %fusion.7, bf16[768,2048]{1,0:T(8,128)(2,1)S(1)} %bitcast.33, bf16[1,2048,512]{2,1,0:T(8,128)(2,1)S(1)} %copy-done), kind=kOutput, calls=%fused_computation.10 | convolution fusion | flops 1616510976 | bytes 10747904 | tf_op jit(solution)/shard_map/dot_general | solution.py:644
  59.2 1.8 %fusion = f32[768,2048]{1,0:T(8,128)S(1)} fusion(bf16[768,512]{1,0:T(8,128)(2,1)S(1)} %get-tuple-element.32.gate_ref, bf16[1,2048,512]{2,1,0:T(8,128)(2,1)S(1)} %copy-done.12), kind=kOutput, calls=%fused_computation.1 | convolution fusion | flops 1610612736 | bytes 9175040 | tf_op jit(solution)/shard_map/dot_general | solution.py:655
  61.0 0.0 copy-start.2
  61.0 0.0 copy-start.3
  61.1 0.0 copy-start.5
  61.1 0.0 copy-start.7
  61.1 0.0 copy-start.9
  61.1 1.9 %add_convert_fusion = bf16[768,2048]{1,0:T(8,128)(2,1)S(1)} fusion(f32[768,2048]{1,0:T(8,128)S(1)} %fusion, bf16[768,512]{1,0:T(8,128)(2,1)S(1)} %get-tuple-element.33.up_ref, bf16[1,2048,512]{2,1,0:T(8,128)(2,1)S(1)} %copy-done), kind=kOutput, calls=%fused_computation | convolution fusion | flops 1613758464 | bytes 12320768 | tf_op jit(solution)/shard_map/dot_general | solution.py:658
  63.0 0.0 copy-done.2
  63.0 0.0 copy-done.3
  63.0 0.0 copy-done.5
  63.0 0.0 copy-done.7
  63.0 0.0 copy-done.9
  63.0 44.7 %shard_map.172 = (bf16[2048,512]{1,0:T(8,128)(2,1)S(1)}, bf16[2048,512]{1,0:T(8,128)(2,1)S(1)}, bf16[512,2048]{1,0:T(8,128)(2,1)S(1)}, f32[256,256]{1,0:T(8,128)...) custom-call(bf16[2,4,96,2048]{3,2,1,0:T(8,128)(2,1)S(1)} %bitcast.31, ...), custom_call_target="tpu_custom_call" | custom-call | tf_op jit(solution)/shard_map/pallas_call | solution.py:522
  107.8 1.3 %copy.26 = bf16[1,2048,512]{2,1,0:T(8,128)(2,1)} copy(bf16[1,2048,512]{2,1,0:T(8,128)(2,1)S(1)} %bitcast.39) | data formatting | bytes 4194304
  109.1 1.3 %copy.27 = bf16[1,2048,512]{2,1,0:T(8,128)(2,1)} copy(bf16[1,2048,512]{2,1,0:T(8,128)(2,1)S(1)} %bitcast.38) | data formatting | bytes 4194304
  110.4 1.3 %copy.28 = bf16[1,512,2048]{2,1,0:T(8,128)(2,1)} copy(bf16[1,512,2048]{2,1,0:T(8,128)(2,1)S(1)} %bitcast.37) | data formatting | bytes 4194304
  111.7 0.7 copy.29
  112.4 0.6 copy.30
  113.1 0.6 copy.31
  113.7 0.6 copy.32
  (1 shorter events, 0.0 us)
Async XLA Ops:
  0.6 56.1 %copy-start = (bf16[1,2048,512]{2,1,0:T(8,128)(2,1)S(1)}, bf16[1,2048,512]{2,1,0:T(8,128)(2,1)}, u32[]{:S(2)}) copy-start(bf16[1,2048,512]{2,1,0:T(8,128)(2,1)} %param.17) | copy-start | bytes 6291460
  3.1 1.0 copy-start.1
  4.1 0.8 copy-start.4
  5.0 0.8 copy-start.6
  5.8 1.0 copy-start.8
  6.9 0.7 copy-start.10
  7.5 0.7 copy-start.11
  51.4 3.6 %copy-start.12 = (bf16[1,2048,512]{2,1,0:T(8,128)(2,1)S(1)}, bf16[1,2048,512]{2,1,0:T(8,128)(2,1)}, u32[]{:S(2)}) copy-start(bf16[1,2048,512]{2,1,0:T(8,128)(2,1)} %param.16) | copy-start | bytes 6291460
  61.0 1.9 %copy-start.2 = (bf16[128,2048]{1,0:T(8,128)(2,1)S(1)}, bf16[128,2048]{1,0:T(8,128)(2,1)}, u32[]{:S(2)}) copy-start(bf16[128,2048]{1,0:T(8,128)(2,1)} %cot_hbm.1) | copy-start | bytes 1572868
  61.0 1.9 %copy-start.3 = (bf16[2048,256]{1,0:T(8,128)(2,1)S(1)}, bf16[2048,256]{1,0:T(8,128)(2,1)}, u32[]{:S(2)}) copy-start(bf16[2048,256]{1,0:T(8,128)(2,1)} %weight_hbm.1) | copy-start | bytes 3145732
  61.1 1.9 %copy-start.5 = (bf16[128,256]{1,0:T(8,128)(2,1)S(1)}, bf16[128,256]{1,0:T(8,128)(2,1)}, u32[]{:S(2)}) copy-start(bf16[128,256]{1,0:T(8,128)(2,1)} %inner_ref.1) | copy-start | bytes 196612
  61.1 1.9 %copy-start.7 = (bf16[128,256]{1,0:T(8,128)(2,1)S(1)}, bf16[128,256]{1,0:T(8,128)(2,1)}, u32[]{:S(2)}) copy-start(bf16[128,256]{1,0:T(8,128)(2,1)} %input_ref.1) | copy-start | bytes 196612
  61.1 1.9 %copy-start.9 = (bf16[128,256]{1,0:T(8,128)(2,1)S(1)}, bf16[128,256]{1,0:T(8,128)(2,1)}, u32[]{:S(2)}) copy-start(bf16[128,256]{1,0:T(8,128)(2,1)} %outer_ref.1) | copy-start | bytes 196612
